TPU v7x, 512 devices: a 4x2x32 block of a 4x8x32 slice. The times are simulated.
512 devices in a mesh: grp: 2 (over y), sp: 64 (over z, core), tp: 4 (over x).
Axes of the slice: x: 4, y: 2, z: 32, core: 2. Of those that a mesh axis runs over, the one named last changes fastest.
The devices are a block of a 4x8x32 slice.
Arguments:
- tokens: bfloat16 [16384, 2048], P(('grp', 'sp'), 'tp'), parts along dimension 0
- mix_gain: bfloat16 [2048], replicated, may hold values from 0.099609375 to 1.8984375
- w_conv_value: bfloat16 [2048, 1024], P('sp', 'tp'), may hold values from -0.125 to 0.125
- w_conv_outer: bfloat16 [2048, 1024], P('sp', 'tp'), may hold values from -0.125 to 0.125
- w_conv_inner: bfloat16 [2048, 1024], P('sp', 'tp'), may hold values from -0.125 to 0.125
- conv_kernel: bfloat16 [3, 1024], P(None, 'tp'), may hold values from -3.5 to 3.5
- w_q_down: bfloat16 [2048, 512], P(None, 'tp'), may hold values from -0.125 to 0.125
- w_kv_down: bfloat16 [2048, 256], P(None, 'tp'), may hold values from -0.125 to 0.125
- w_rope_key: bfloat16 [2048, 32], replicated, may hold values from -0.125 to 0.125
- q_gain: bfloat16 [512], replicated
- kv_gain: bfloat16 [256], replicated, may hold values from 0.099609375 to 1.8984375
- w_q_nope: bfloat16 [512, 1024], P(None, 'tp'), may hold values from -0.25 to 0.25
- w_q_rope: bfloat16 [512, 512], P(None, 'tp'), may hold values from -0.25 to 0.25
- w_k_nope: bfloat16 [256, 1024], P(None, 'tp'), may hold values from -0.375 to 0.375
- w_value: bfloat16 [256, 1024], P(None, 'tp'), may hold values from -0.375 to 0.375
- w_out_conv: bfloat16 [1024, 2048], P('tp'), may hold values from -0.1875 to 0.1875
- w_out_attn: bfloat16 [1024, 2048], P('tp'), may hold values from -1.5 to 1.5
Outputs:
- mixed: bfloat16 [16384, 2048], P(('grp', 'sp'), 'tp'), parts along dimension 0
There are 2 independent parts, one for each index of `grp`. A program takes and returns all parts, laid end to end along the dimension named above; an argument that names none is the same for every part. Nothing has to cross between parts.
All inputs are finite; a program needn't handle non-finite values.
Results may differ from a plain program's by a relative error of at most 0.028.
Values may be sent and summed in bfloat16 or wider, within the bound.
A program may use at most 64 MiB of HBM per device.

v0:
```python
import jax
import jax.numpy as jnp
from jax import lax
from jax.sharding import PartitionSpec as P

D = 2048
NOPE = 64
ROPE = 32
VALUE = 64


EPS = 1e-06
THETA = 10000.0


def sent_together(arrays, axis, dim, along):
    ends, at = ([], 0)
    for a in arrays[:-1]:
        at += a.shape[along]
        ends.append(at)
    both = jnp.concatenate(arrays, axis=along)
    return tuple(jnp.split(lax.all_gather(both, axis, axis=dim, tiled=True), ends, axis=along))


def in_order(tiles, dim):
    tiles = jnp.moveaxis(tiles, 0, dim)
    lengths = tiles.shape
    return tiles.reshape(*lengths[:dim], lengths[dim] * lengths[dim + 1], *lengths[dim + 2 :])


def from_everyone(x, axis):
    copies = jnp.broadcast_to(x, (lax.axis_size(axis), *x.shape))
    return lax.all_to_all(copies, axis, split_axis=0, concat_axis=0, tiled=True)


def gather_directly(x, axis, dim):
    return in_order(from_everyone(x, axis), dim)


def with_halo(x, sides, width):
    for axis, dim in sides:
        size, length = (lax.axis_size(axis), x.shape[dim])
        up = [(i, (i + 1) % size) for i in range(size - 1)]
        down = [(j, i) for i, j in up]
        last = lax.slice_in_dim(x, length - width, length, axis=dim)
        first = lax.slice_in_dim(x, 0, width, axis=dim)
        before = lax.ppermute(last, axis, up)
        after = lax.ppermute(first, axis, down)
        x = jnp.concatenate([before, x, after], axis=dim)
    return x


def one_gather(arrays, axis, dims):
    vector = jnp.concatenate([a.reshape(-1) for a in arrays])
    lines, at, done = (lax.all_gather(vector, axis), 0, [])
    for a, dim in zip(arrays, dims):
        tiles = lines[:, at : at + a.size].reshape(-1, *a.shape)
        done.append(in_order(tiles, dim))
        at += a.size
    return tuple(done)


def cut_along(x, dim, length):
    before, after = (x.shape[:dim], x.shape[dim + 1 :])
    return jnp.moveaxis(x.reshape(*before, length, -1, *after), dim, 0)


def summed_on_arrival(x, axis, dim):
    tiles = cut_along(x, dim, lax.axis_size(axis))
    arrived = lax.all_to_all(tiles, axis, split_axis=0, concat_axis=0, tiled=True)
    return arrived.astype(jnp.float32).sum(axis=0)


def rms_scale(values):
    return lax.rsqrt(jnp.mean(values * values, axis=-1, keepdims=True) + EPS)


def angles(positions, width):
    inverse = THETA ** (-jnp.arange(0, width, 2, dtype=jnp.float32) / width)
    phase = positions[:, None] * inverse[None, :]
    phase = jnp.concatenate([phase, phase], axis=-1)
    return (jnp.cos(phase), jnp.sin(phase))


def turned(values, cosine, sine):
    half = values.shape[-1] // 2
    first = values[..., :half]
    second = values[..., half:]
    return values * cosine + jnp.concatenate([-second, first], axis=-1) * sine


def block_rows(count):
    for candidate in range(min(count, 1024), 0, -1):
        if count % candidate == 0 and candidate % 128 == 0:
            return candidate
    for candidate in range(min(count, 1024), 0, -1):
        if count % candidate == 0:
            return candidate
    return count


def per_device(
    tokens,
    mix_gain,
    w_conv_value,
    w_conv_outer,
    w_conv_inner,
    conv_kernel,
    w_q_down,
    w_kv_down,
    w_rope_key,
    q_gain,
    kv_gain,
    w_q_nope,
    w_q_rope,
    w_k_nope,
    w_value,
    w_out_conv,
    w_out_attn,
):
    f32 = jnp.float32
    bf16 = jnp.bfloat16
    rows = tokens.shape[0]
    conv_value_w, conv_outer_w, conv_inner_w = sent_together(
        (w_conv_value, w_conv_outer, w_conv_inner), "sp", 0, 1
    )
    matrices = (conv_value_w, conv_outer_w, conv_inner_w, w_q_down, w_kv_down, w_rope_key)
    gain = mix_gain.astype(f32)
    piece_f = gather_directly(tokens, "tp", 1).astype(f32)
    scaled = (piece_f * gain).astype(bf16)
    updated = tuple((jnp.dot(scaled, matrix, preferred_element_type=f32) for matrix in matrices))
    squares = jnp.sum(piece_f * piece_f, axis=1)
    row_scale = lax.rsqrt(squares / D + EPS)[:, None]
    conv_value, conv_outer, conv_inner, q_part, kv_part, rope_raw = [
        (row_scale * total).astype(bf16) for total in updated
    ]
    gated = (conv_inner.astype(f32) * conv_value.astype(f32)).astype(bf16)
    padded = with_halo(gated, (("sp", 0),), 1).astype(f32)
    kernel = conv_kernel.astype(f32)
    conv_out = padded[:-2] * kernel[0] + padded[1:-1] * kernel[1] + padded[2:] * kernel[2]
    y_conv = (conv_outer.astype(f32) * conv_out).astype(bf16)
    q_latent, kv_latent = one_gather((q_part, kv_part), "tp", (1, 1))
    q_float = q_latent.astype(f32)
    q_normed = (q_float * rms_scale(q_float) * q_gain.astype(f32)).astype(bf16)
    kv_float = kv_latent.astype(f32)
    kv_normed = (kv_float * rms_scale(kv_float) * kv_gain.astype(f32)).astype(bf16)
    heads = w_q_nope.shape[1] // NOPE
    positions = (lax.axis_index("sp") * rows + jnp.arange(rows, dtype=jnp.int32)).astype(f32)
    cosine, sine = angles(positions, ROPE)
    q_nope = (
        jnp.dot(q_normed, w_q_nope, preferred_element_type=f32)
        .astype(bf16)
        .reshape(rows, heads, NOPE)
    )
    q_rope_raw = jnp.dot(q_normed, w_q_rope, preferred_element_type=f32).reshape(rows, heads, ROPE)
    q_rope = turned(q_rope_raw, cosine[:, None, :], sine[:, None, :]).astype(bf16)
    k_rope = turned(rope_raw.astype(f32), cosine, sine).astype(bf16)
    factor = (NOPE + ROPE) ** (-0.5)

    def attend(state, key_block, value_block, rope_block):
        peak, total, summed = state
        count = key_block.shape[0]
        keys3 = key_block.reshape(count, heads, NOPE)
        values3 = value_block.reshape(count, heads, VALUE)
        scores = jnp.einsum("qhd,khd->qhk", q_nope, keys3, preferred_element_type=f32)
        scores = scores + jnp.einsum("qhr,kr->qhk", q_rope, rope_block, preferred_element_type=f32)
        scores = scores * factor
        new_peak = jnp.maximum(peak, jnp.max(scores, axis=-1))
        fade = jnp.exp(peak - new_peak)
        weights = jnp.exp(scores - new_peak[..., None])
        total = total * fade + jnp.sum(weights, axis=-1)
        summed = summed * fade[..., None] + jnp.einsum(
            "qhk,khd->qhd", weights.astype(bf16), values3, preferred_element_type=f32
        )
        return (new_peak, total, summed)

    start_state = (
        jnp.full((rows, heads), -jnp.inf, f32),
        jnp.zeros((rows, heads), f32),
        jnp.zeros((rows, heads, VALUE), f32),
    )
    latent, rope_keys = sent_together((kv_normed, k_rope), "sp", 0, 1)
    size = block_rows(latent.shape[0])
    count = latent.shape[0] // size

    def one_block(carry, blocks):
        latent_block, rope_block = blocks
        key_block = jnp.dot(latent_block, w_k_nope, preferred_element_type=f32).astype(bf16)
        value_block = jnp.dot(latent_block, w_value, preferred_element_type=f32).astype(bf16)
        return (attend(carry, key_block, value_block, rope_block), None)

    carry, ignored = lax.scan(
        one_block,
        start_state,
        (
            latent.reshape(count, size, latent.shape[1]),
            rope_keys.reshape(count, size, rope_keys.shape[1]),
        ),
    )
    peak, total, summed = carry
    y_attn = (summed / total[..., None]).astype(bf16).reshape(rows, heads * VALUE)
    partial_sum = jnp.dot(y_conv, w_out_conv, preferred_element_type=f32) + jnp.dot(
        y_attn, w_out_attn, preferred_element_type=f32
    )
    return summed_on_arrival(partial_sum.astype(jnp.bfloat16), "tp", 1).astype(bf16)


def solution(mesh):
    placed = (
        P(("grp", "sp"), "tp"),
        P(),
        P("sp", "tp"),
        P("sp", "tp"),
        P("sp", "tp"),
        P(None, "tp"),
        P(None, "tp"),
        P(None, "tp"),
        P(),
        P(),
        P(),
        P(None, "tp"),
        P(None, "tp"),
        P(None, "tp"),
        P(None, "tp"),
        P("tp", None),
        P("tp", None),
    )
    return jax.shard_map(
        per_device, mesh=mesh, in_specs=placed, out_specs=P(("grp", "sp"), "tp"), check_vma=False
    )
```

profile of v0, /device:TPU:33, one launch (start us, length us, event | category | flops | bytes accessed | tf_op | source)
XLA Modules:
  0.0 386.4 jit_solution(4682824905297936708)
XLA Ops:
  6.6 1.5 pad_maximum_fusion.1
  10.1 5.1 %all-to-all-start = ((bf16[4,128,512]{1,2,0:T(8,128)(2,1)}), bf16[4,128,512]{1,2,0:T(8,128)(2,1)S(1)}, u32[]{:S(2)}, u32[]{:S(2)}) async-start(bf16[4,128,512]{1,2,0:T(8,128)(2,1)} %broadcast_in_dim.8), calls=%async_computation | async-start | bytes 1048576 | tf_op jit(solution)/shard_map/all_to_all | solution.py:33
  15.3 6.8 %all-to-all-done = bf16[4,128,512]{1,2,0:T(8,128)(2,1)S(1)} async-done(((bf16[4,128,512]{1,2,0:T(8,128)(2,1)}), bf16[4,128,512]{1,2,0:T(8,128)(2,1)S(1)}, u32[]{:S(2)}, u32[]{:S(2)}) %all-to-all-start) | async-done | bytes 524320 | tf_op jit(solution)/shard_map/all_to_all | solution.py:33
  23.6 9.3 %all-gather = bf16[98304]{0:T(1024)(128)(2,1)S(1)} all-gather(bf16[24576]{0:T(1024)(128)(2,1)S(1)} %pad_maximum_fusion.2), channel_id=2, replica_groups=mesh['grp'=2,'sp'=64,'tp'=4] {'tp'}, dimensions={0}, use_global_device_ids=true | all-gather | bytes 245760 | tf_op jit(solution)/shard_map/all_gather | solution.py:55
  36.1 135.4 %all-gather.4.cloned.1.call-done = bf16[2048,768]{1,0:T(8,128)(2,1)} async-done(((bf16[32,768]{1,0:T(8,128)(2,1)}), bf16[2048,768]{1,0:T(8,128)(2,1)}) %all-gather.4.cloned.1.call-update) | async-done | bytes 3145744 | tf_op jit(solution)/shard_map/all_gather | solution.py:22
  171.5 1.6 fusion.26
  173.1 1.6 fusion.24
  174.7 2.1 collective-permute-start
  176.8 2.3 collective-permute-start.1
  179.2 2.5 collective-permute-done.1
  181.7 2.0 fusion.27
  183.8 124.1 %all-gather.6.cloned.1.call-done = bf16[8192,288]{0,1:T(8,128)(2,1)} async-done(((bf16[128,288]{0,1:T(8,128)(2,1)}), bf16[8192,288]{0,1:T(8,128)(2,1)}) %all-gather.6.cloned.1.call-update) | async-done | bytes 4718608 | tf_op jit(solution)/shard_map/all_gather | solution.py:22
  307.8 4.6 %split.23 = bf16[8192,256]{0,1:T(8,128)(2,1)} slice(bf16[8192,288]{0,1:T(8,128)(2,1)} %all-gather.6.cloned.1.call-done), slice={[0:8192], [0:256]} | slice | bytes 8388608 | tf_op jit(solution)/shard_map/split | solution.py:22
  312.5 6.5 %copy.74 = bf16[8192,256]{1,0:T(8,128)(2,1)} copy(bf16[8192,256]{0,1:T(8,128)(2,1)} %split.23) | data formatting | bytes 8388608
  320.1 44.3 %while.15 = (s32[]{:T(128)}, f32[128,4]{0,1:T(4,128)S(1)}, f32[128,4]{0,1:T(4,128)S(1)}, f32[128,4,64]{0,2,1:T(8,128)S(1)}, bf16[8,1024,256]{2,1,0:T(8,128)(2,1)...) while((s32[]{:T(128)}, f32[128,4]{0,1:T(4,128)S(1)}, ...), condition=%wide.region_7.8_spmd.clone, body=%wide.region_4.7_spmd.clone.sunk | while | flops 440502784 | bytes 14352533 | solution.py:192
  321.4 1.4 convolution_convert_fusion.5
  325.6 1.4 convolution_convert_fusion.6
  327.0 1.4 convolution_convert_fusion.5
  331.1 1.4 convolution_convert_fusion.6
  332.5 1.4 convolution_convert_fusion.5
  336.7 1.4 convolution_convert_fusion.6
  349.2 1.4 convolution_convert_fusion.5
  364.4 1.6 fusion.16
  366.0 12.8 %all_to_all.10 = bf16[4,128,512]{2,1,0:T(8,128)(2,1)S(1)} all-to-all(bf16[4,128,512]{2,1,0:T(8,128)(2,1)S(1)} %bitcast.140), channel_id=1, replica_groups=mesh['grp'=2,'sp'=64,'tp'=4] {'tp'}, dimensions={0} | all-to-all | bytes 1048576 | tf_op jit(solution)/shard_map/all_to_all | solution.py:70
  (149 shorter events, 42.7 us)
Async XLA Ops:
  6.5 175.2 %copy-start = (bf16[256,2048]{1,0:T(8,128)(2,1)S(1)}, bf16[256,2048]{1,0:T(8,128)(2,1)}, u32[]{:S(2)}) copy-start(bf16[256,2048]{1,0:T(8,128)(2,1)} %param.34) | copy-start | bytes 3145732
  6.6 8.6 %copy-start.11 = (bf16[256]{0:T(256)(128)(2,1)S(1)}, bf16[256]{0:T(256)(128)(2,1)}, u32[]{:S(2)}) copy-start(bf16[256]{0:T(256)(128)(2,1)} %param.29) | copy-start | bytes 1540
  6.6 8.6 %copy-start.9 = (bf16[2048]{0:T(1024)(128)(2,1)S(1)}, bf16[2048]{0:T(1024)(128)(2,1)}, u32[]{:S(2)}) copy-start(bf16[2048]{0:T(1024)(128)(2,1)} %param.20) | copy-start | bytes 12292
  6.6 16.2 %copy-start.5 = (bf16[2048,64]{0,1:T(8,128)(2,1)S(1)}, bf16[2048,64]{0,1:T(8,128)(2,1)}, u32[]{:S(2)}) copy-start(bf16[2048,64]{0,1:T(8,128)(2,1)} %param.26) | copy-start | bytes 786436
  6.6 164.9 %all-gather.4.cloned.1.call-start = ((), (), s32[]{:S(2)}) async-start(), calls=%async_computation.2 | async-start | bytes 3194880 | tf_op jit(solution)/shard_map/all_gather | solution.py:22
  9.2 14.0 %copy-start.3 = (bf16[2048,128]{1,0:T(8,128)(2,1)S(1)}, bf16[2048,128]{1,0:T(8,128)(2,1)}, u32[]{:S(2)}) copy-start(bf16[2048,128]{1,0:T(8,128)(2,1)} %param.25) | copy-start | bytes 1572868
  10.1 12.1 %all-to-all-start = ((bf16[4,128,512]{1,2,0:T(8,128)(2,1)}), bf16[4,128,512]{1,2,0:T(8,128)(2,1)S(1)}, u32[]{:S(2)}, u32[]{:S(2)}) async-start(bf16[4,128,512]{1,2,0:T(8,128)(2,1)} %broadcast_in_dim.8), calls=%async_computation | async-start | bytes 1048576 | tf_op jit(solution)/shard_map/all_to_all | solution.py:33
  15.2 292.7 %all-gather.6.cloned.1.call-start = ((), (), s32[]{:S(2)}) async-start(), calls=%async_computation.3 | async-start | bytes 4792320 | tf_op jit(solution)/shard_map/all_gather | solution.py:22
  22.8 10.9 %copy-start.7 = (bf16[2048,32]{0,1:T(8,128)(2,1)S(1)}, bf16[2048,32]{0,1:T(8,128)(2,1)}, u32[]{:S(2)}) copy-start(bf16[2048,32]{0,1:T(8,128)(2,1)} %param.27) | copy-start | bytes 393220
  23.2 11.5 %copy-start.6 = (bf16[512,128]{1,0:T(8,128)(2,1)S(1)}, bf16[512,128]{1,0:T(8,128)(2,1)}, u32[]{:S(2)}) copy-start(bf16[512,128]{1,0:T(8,128)(2,1)} %param.31) | copy-start | bytes 393220
  23.2 11.6 %copy-start.10 = (bf16[512]{0:T(512)(128)(2,1)S(1)}, bf16[512]{0:T(512)(128)(2,1)}, u32[]{:S(2)}) copy-start(bf16[512]{0:T(512)(128)(2,1)} %param.28) | copy-start | bytes 3076
  23.3 11.6 %copy-start.8 = (bf16[3,256]{1,0:T(4,128)(2,1)S(1)}, bf16[3,256]{1,0:T(4,128)(2,1)}, u32[]{:S(2)}) copy-start(bf16[3,256]{1,0:T(4,128)(2,1)} %param.24) | copy-start | bytes 4612
  33.8 2.0 copy-start.4
  174.7 4.5 %collective-permute-start = (bf16[1,256]{1,0:T(2,128)(2,1)S(1)}, bf16[1,256]{1,0:T(2,128)(2,1)S(1)}, u32[]{:S(2)}, u32[]{:S(2)}) collective-permute-start(bf16[1,256]{1,0:T(2,128)(2,1)S(1)} %get-tuple-element.179), channel_id=1, source_target_pairs={{0,4},{4,8},{8,12},{12,16},{16,20},{20,24},{24,28},{28,32},{32,36}... | collective-permute-start | bytes 1544 | tf_op jit(solution)/shard_map/ppermute | solution.py:47
  176.8 4.9 %collective-permute-start.1 = (bf16[1,256]{1,0:T(2,128)(2,1)S(1)}, bf16[1,256]{1,0:T(2,128)(2,1)S(1)}, u32[]{:S(2)}, u32[]{:S(2)}) collective-permute-start(bf16[1,256]{1,0:T(2,128)(2,1)S(1)} %get-tuple-element.180), channel_id=1, source_target_pairs={{4,0},{8,4},{12,8},{16,12},{20,16},{24,20},{28,24},{32,28},{36,32}... | collective-permute-start | bytes 1544 | tf_op jit(solution)/shard_map/ppermute | solution.py:48
  312.5 6.5 %slice-start = ((bf16[8192,288]{0,1:T(8,128)(2,1)}), bf16[8192,32]{0,1:T(8,128)(2,1)S(1)}, s32[]{:S(2)}) async-start(bf16[8192,288]{0,1:T(8,128)(2,1)} %all-gather.6.cloned.1.call-done), calls=%async_computation.4 | async-start | bytes 1048576 | tf_op jit(solution)/shard_map/split | solution.py:22
  319.0 0.9 copy-start.1
  319.0 1.1 copy-start.2
Sparse Core Ops, SparseCore 0:
  9.5 161.9 all-gather.3
  173.6 134.2 all-gather.5
where the time goes:
time: 388 us; the launch traced here: 386 us
  waiting for transfers between devices  269 us (69%)
  matrix products  49.2 us (13%)
  blocking collectives  22.1 us (6%)
  local copies, waits for them, and re-layouts  15.4 us (4%)
  between operations  13.9 us (4%)
  starting transfers between devices  9.56 us (2%)
  other arithmetic  6.97 us (2%)
    all_gather x2, waiting for transfers between devices, sent_together(): lax.all_gather(both, axis, axis=dim, tiled=True)  259 us
    all_to_all x1, blocking collectives, summed_on_arrival(): lax.all_to_all(tiles, axis, split_axis=0, concat_axis=0, tiled=True)  12.8 us
    dot_general x8, matrix products, one_block(): jnp.dot(latent_block, w_k_nope, preferred_element_type=f32).astype(bf16)  11.1 us
    dot_general x8, matrix products, one_block(): jnp.dot(latent_block, w_value, preferred_element_type=f32).astype(bf16)  11.1 us
    dot_general x8, matrix products, attend(): jnp.einsum('qhr,kr->qhk', q_rope, rope_block, preferred_element_type=f32)  10.5 us
    all_gather x1, blocking collectives, one_gather(): lines, at, done = (lax.all_gather(vector, axis), 0, [])  9.29 us
    unnamed x28, local copies, waits for them, and re-layouts  7.92 us
  transfers between devices with their start and end apart: 5, of which 4 were waited for; matrix products, arithmetic and copies ran while one was open for 3% of the time, Pallas kernels for 0%

commit v1 on v0

v1 whole, which is shorter than its diff:
```python
import functools
import math

import jax
import jax.numpy as jnp
from jax import lax
from jax.experimental import pallas as pl
from jax.experimental.pallas import tpu as pltpu
from jax.sharding import PartitionSpec as P

NOPE = 64
ROPE = 32
VALUE = 64
EPS = 1e-06
THETA = 10000.0
LOG2E = 1.4426950408889634
MESH = pl.DeviceIdType.MESH
F32 = jnp.float32
BF16 = jnp.bfloat16
W_AHEAD = 3


def dot_f32(a, b, contract=((1,), (0,))):
    return lax.dot_general(a, b, (contract, ((), ())), preferred_element_type=F32)


def kernel(
    SP, X,
    tokens, mix_gain, wv, wo, wi, conv_kernel, wqd, wkvd, wrk, q_gain, kv_gain,
    wqn, wqr, wkn, wval, woc, woa,
    out,
    wbuf, tok, scaled, wqd_v, wkvd_v, wrk_v, wd, wqn_v, wqr_v, wkn_v, wval_v, wval_t, wout,
    qbuf, qmine, qpart, qz, kvbuf, rope_scr, cs_scr, qg_col, kvg_col, rs_scr,
    o_acc, m_acc, l_acc, o_send, o_recv, gated, halo, yconv, rs_send, rs_recv,
    loc, tk_s, tk_r, q_s, q_r, qp_s, qp_r, kz_s, kz_r, kx_s, kx_r, wz_s, wz_r, wp_s, wp_r,
    o_s, o_r, h_s, h_r, r_s, r_r,
):
    Z = SP // 2
    HALF = Z // 2
    T = tokens.shape[0]
    DX = tokens.shape[1]
    D = DX * X
    H = wqn.shape[1] // NOPE
    sp = lax.axis_index("sp")
    x = lax.axis_index("tp")
    z = lax.div(sp, 2)
    c = lax.rem(sp, 2)
    up = lax.rem(z + 1, Z)
    dn = lax.rem(z + Z - 1, Z)
    xr = lax.rem(x + 1, X)
    xl = lax.rem(x + X - 1, X)
    xo = lax.rem(x + 2, X)
    to_up = {"sp": up * 2 + c}
    to_dn = {"sp": dn * 2 + c}
    partner = {"sp": z * 2 + 1 - c}
    to_xr, to_xl, to_xo = {"tp": xr}, {"tp": xl}, {"tp": xo}
    prev_sp = lax.rem(sp + SP - 1, SP)
    next_sp = lax.rem(sp + 1, SP)
    other_chip = {"sp": jnp.where(c == 0, prev_sp, next_sp)}

    def remote(src, dst, ssem, rsem, dev):
        return pltpu.make_async_remote_copy(
            src_ref=src, dst_ref=dst, send_sem=ssem, recv_sem=rsem, device_id=dev, device_id_type=MESH
        )

    local = []
    def bring(src, dst):
        cp = pltpu.make_async_copy(src, dst, loc.at[len(local)])
        local.append(cp)
        cp.start()
        return cp

    conv_cp = [bring(w, wbuf.at[i, z, c]) for i, w in enumerate((wv, wo, wi))]
    tok_cp = bring(tokens, tok.at[x])
    down_cp = [bring(wqd, wqd_v), bring(wkvd, wkvd_v), bring(wrk, wrk_v)]
    up_cp = [bring(wqn, wqn_v), bring(wqr, wqr_v), bring(wkn, wkn_v), bring(wval, wval_v)]
    NC = woc.shape[0]
    out_cp = [bring(woc, wout.at[pl.ds(0, NC)]), bring(woa, wout.at[pl.ds(NC, woa.shape[0])])]

    barrier = pltpu.get_barrier_semaphore()
    for dev in (to_up, to_dn, partner, to_xr, to_xl, to_xo, other_chip):
        pl.semaphore_signal(barrier, inc=1, device_id=dev, device_id_type=MESH)
    pl.semaphore_wait(barrier, 7)

    h = T // 2
    lo, hi = pl.ds(0, h), pl.ds(h, h)

    def tok_copy(k, piece, rows, dev, first):
        src = tokens.at[rows] if first else tok.at[piece, rows]
        return remote(src, tok.at[piece, rows], tk_s.at[k], tk_r.at[k], dev)

    tok_sends = [
        tok_copy(0, x, lo, to_xr, True), tok_copy(2, x, hi, to_xl, True),
        tok_copy(1, x, hi, to_xr, True), tok_copy(3, x, lo, to_xl, True),
    ]
    for cp in tok_sends:
        cp.start()

    def w_z(slot, d, way, dev):
        return remote(wbuf.at[:, slot, c], wbuf.at[:, slot, c], wz_s.at[way, d], wz_r.at[slot], dev)

    def w_p(slot, core):
        return remote(wbuf.at[:, slot, core], wbuf.at[:, slot, core], wp_s.at[slot], wp_r.at[slot], partner)

    for cp in conv_cp:
        cp.wait()
    w_z(z, 0, 0, to_up).start()
    w_z(z, 0, 1, to_dn).start()
    w_p(z, c).start()

    def when(cond, fn):
        if isinstance(cond, bool):
            if cond:
                fn()
        else:
            pl.when(cond)(fn)

    def w_step(k):
        def go_up():
            slot = lax.rem(z - k + Z, Z)
            w_z(slot, k, 0, to_up).wait_recv()
            when(k < HALF, lambda: w_z(slot, k, 0, to_up).start())
            w_p(slot, c).start()

        def go_dn():
            slot = lax.rem(z + k, Z)
            w_z(slot, k, 1, to_dn).wait_recv()
            when(k < HALF - 1, lambda: w_z(slot, k, 1, to_dn).start())
            w_p(slot, c).start()

        when(k <= HALF, go_up)
        when(k <= HALF - 1, go_dn)

    for cp in down_cp:
        cp.wait()
    wd[:, : wqd.shape[1]] = wqd_v[...]
    nk, nr = wkvd.shape[1], wrk.shape[1]
    wd[:, wqd.shape[1] :] = jnp.concatenate(
        [wkvd_v[...], wrk_v[...], jnp.zeros((D, 128 - nk - nr), BF16)], axis=1
    )
    rows16 = lax.broadcasted_iota(jnp.int32, (ROPE, T), 0)
    freq = jnp.where(rows16 >= ROPE // 2, rows16 - ROPE // 2, rows16).astype(F32) * 2.0
    inverse = jnp.exp(freq * (-math.log(THETA) / ROPE))
    phase = (sp * T + lax.broadcasted_iota(jnp.int32, (ROPE, T), 1)).astype(F32) * inverse
    cs_scr[0] = jnp.cos(phase)
    cs_scr[1] = jnp.sin(phase)
    qg_col[...] = jnp.transpose(jnp.broadcast_to(q_gain[...].astype(F32), (128, q_gain.shape[1])))
    kvg_col[...] = jnp.transpose(jnp.broadcast_to(kv_gain[...].astype(F32), (128, kv_gain.shape[1])))
    qz[...] = jnp.zeros(qz.shape, BF16)
    o_acc[...] = jnp.zeros(o_acc.shape, F32)
    m_acc[...] = jnp.full(m_acc.shape, -jnp.inf, F32)
    l_acc[...] = jnp.zeros(l_acc.shape, F32)
    for cp in up_cp:
        cp.wait()
    wval_t[...] = jnp.transpose(wval_v[...].astype(F32)).astype(BF16)

    tok_copy(0, xl, lo, to_xr, False).wait_recv()
    tok_copy(4, xl, lo, to_xr, False).start()
    tok_copy(2, xr, hi, to_xl, False).wait_recv()
    tok_copy(5, xr, hi, to_xl, False).start()
    tok_copy(1, xl, hi, to_xr, False).wait_recv()
    tok_copy(3, xr, lo, to_xl, False).wait_recv()
    w_step(1)
    tok_copy(4, xo, lo, to_xr, False).wait_recv()
    tok_copy(5, xo, hi, to_xl, False).wait_recv()
    tok_cp.wait()

    down = jnp.zeros((T, wd.shape[1]), F32)
    squares = jnp.zeros((T, 1), F32)
    for j in range(X):
        t = tok[j].astype(F32)
        s = (t * mix_gain[:, j * DX : (j + 1) * DX].astype(F32)).astype(BF16)
        scaled[:, j * DX : (j + 1) * DX] = s
        squares += jnp.sum(t * t, axis=1, keepdims=True)
        down += dot_f32(s, wd[j * DX : (j + 1) * DX, :])
    row_scale = lax.rsqrt(squares / D + EPS)
    rs_scr[...] = jnp.broadcast_to(row_scale, rs_scr.shape)
    down_t = jnp.transpose(down * row_scale)
    nq = wqd.shape[1]
    kv_rows = pl.ds(0, nk)
    kvbuf[z, x, kv_rows, :] = down_t[nq : nq + nk].astype(BF16)

    def turned(v, cosine, sine):
        half = ROPE // 2
        return v * cosine + jnp.concatenate([-v[half:], v[:half]], axis=0) * sine

    raw = down_t[nq + nk : nq + nk + nr].astype(BF16).astype(F32)
    rope_scr[...] = turned(raw, cs_scr[0], cs_scr[1])
    RX = ROPE // X
    mine = rope_scr[pl.ds(pl.multiple_of(x * RX, RX), RX), :]
    kvbuf[z, x, pl.ds(nk, 2 * RX), :] = jnp.concatenate([mine, jnp.zeros((RX, T), F32)], axis=0).astype(BF16)

    def k_z(slot, d, way, dev):
        return remote(kvbuf.at[slot, x], kvbuf.at[slot, x], kz_s.at[way, d], kz_r.at[slot], dev)

    def k_x(slot, piece, kind, dev):
        return remote(kvbuf.at[slot, piece], kvbuf.at[slot, piece], kx_s.at[slot, kind], kx_r.at[slot, kind], dev)

    k_z(z, 0, 0, to_up).start()
    k_z(z, 0, 1, to_dn).start()
    k_x(z, x, 0, to_xr).start()
    k_x(z, x, 1, to_xl).start()

    qbuf[x] = down_t[:nq].astype(BF16)

    def q_copy(kind, piece, dev):
        return remote(qbuf.at[piece], qbuf.at[piece], q_s.at[kind], q_r.at[kind], dev)

    q_sends = [q_copy(2, x, to_xo), q_copy(0, x, to_xr), q_copy(1, x, to_xl)]
    for cp in q_sends:
        cp.start()
    for k in range(2, W_AHEAD + 1):
        if k <= HALF:
            w_step(k)

    factor = (NOPE + ROPE) ** (-0.5) * LOG2E
    q_exchange = remote(qmine, qpart, qp_s.at[0], qp_r.at[0], partner)

    def make_q():
        q_copy(0, xl, to_xr).wait_recv()
        q_copy(1, xr, to_xl).wait_recv()
        q_copy(2, xo, to_xo).wait_recv()
        qf = qbuf[...].reshape(X * nq, T).astype(F32)
        scale = lax.rsqrt(jnp.mean(qf * qf, axis=0, keepdims=True) + EPS)
        qn = (qf * scale * qg_col[...]).astype(BF16)
        nope = dot_f32(wqn_v[...], qn, ((0,), (0,))) * factor
        qmine[: H * NOPE, :] = nope.astype(BF16)
        rope = dot_f32(wqr_v[...], qn, ((0,), (0,)))
        for i in range(H):
            r = turned(rope[i * ROPE : (i + 1) * ROPE], cs_scr[0], cs_scr[1]) * factor
            qmine[H * NOPE + i * ROPE : H * NOPE + (i + 1) * ROPE, :] = r.astype(BF16)
        q_exchange.start()

    def place_q():
        q_exchange.wait_recv()
        for i in range(H):
            p, e = divmod(i, 2)
            for src, at in ((qmine, 0), (qpart, T)):
                cols = slice(e * 2 * T + at, e * 2 * T + at + T)
                qz[p, e * NOPE : (e + 1) * NOPE, cols] = src[i * NOPE : (i + 1) * NOPE, :]
                qz[p, 2 * NOPE : 2 * NOPE + ROPE, cols] = src[H * NOPE + i * ROPE : H * NOPE + (i + 1) * ROPE, :]

    def keys(slot):
        lat = kvbuf[slot, :, :nk, :].reshape(X * nk, T).astype(F32)
        rope = kvbuf[slot, :, nk : nk + 2 * RX, :].astype(F32)[:, :RX].reshape(ROPE, T)
        return lat, rope

    def chunk(slot_a, slot_b):
        la, ra = keys(slot_a)
        lb, rb = keys(slot_b)
        lat = jnp.concatenate([la, lb], axis=1)
        scale = lax.rsqrt(jnp.mean(lat * lat, axis=0, keepdims=True) + EPS)
        gain = kvg_col[...]
        n = (lat * scale * jnp.concatenate([gain, gain], axis=1)).astype(BF16)
        kn = dot_f32(n, wkn_v[...], ((0,), (0,))).astype(BF16)
        rope = jnp.concatenate([ra, rb], axis=1)
        kr = jnp.transpose(jnp.concatenate([rope, jnp.zeros((128 - ROPE, 2 * T), F32)], axis=0)).astype(BF16)
        vt = dot_f32(wval_t[...], n).astype(BF16)
        for p in range(H // 2):
            kp = jnp.concatenate([kn[:, p * 128 : (p + 1) * 128], kr], axis=1)
            s = dot_f32(kp, qz[p])
            old = m_acc[p]
            new = jnp.maximum(old, jnp.max(s, axis=0, keepdims=True))
            m_acc[p] = new
            fade = jnp.exp2(old - new)
            w = jnp.exp2(s - new)
            l_acc[p] = l_acc[p] * fade + jnp.sum(w, axis=0, keepdims=True)
            wb = w.astype(BF16)
            for e in range(2):
                i = 2 * p + e
                cols = slice(e * 2 * T, (e + 1) * 2 * T)
                o_acc[i] = o_acc[i] * fade[:, cols] + dot_f32(vt[i * VALUE : (i + 1) * VALUE], wb[:, cols])

    def halo_copy(k, dev):
        rows = pl.ds(0, 8) if k == 1 else pl.ds(T - 8, 8)
        return remote(gated.at[rows], halo.at[k], h_s.at[k], h_r.at[k], dev)

    to_next, to_prev = {"sp": next_sp}, {"sp": prev_sp}

    def conv_gates():
        def got(s, _):
            w_p(s, 1 - c).wait_recv()
            return 0
        lax.fori_loop(0, Z, got, 0)
        def project(i):
            w = wbuf[i].reshape(D, wbuf.shape[-1])
            return (dot_f32(scaled[...], w) * rs_scr[:, 0:1]).astype(BF16).astype(F32)
        inner = project(2)
        value = project(0)
        gated[...] = (inner * value).astype(BF16).astype(F32)
        halo_copy(0, to_next).start()
        halo_copy(1, to_prev).start()
        yconv[...] = project(1)

    def step(d, _):
        def up_in():
            slot = lax.rem(z - d + Z, Z)
            k_z(slot, d, 0, to_up).wait_recv()
            pl.when(d < HALF)(lambda: k_z(slot, d, 0, to_up).start())
            k_x(slot, x, 0, to_xr).start()
            k_x(slot, x, 1, to_xl).start()

        def dn_in():
            slot = lax.rem(z + d, Z)
            k_z(slot, d, 1, to_dn).wait_recv()
            pl.when(d < HALF - 1)(lambda: k_z(slot, d, 1, to_dn).start())
            k_x(slot, x, 0, to_xr).start()
            k_x(slot, x, 1, to_xl).start()

        pl.when(d <= HALF)(up_in)
        pl.when(d <= HALF - 1)(dn_in)

        e = d - 1

        def relay_up():
            slot = lax.rem(z - e + Z, Z)
            k_x(slot, xl, 0, to_xr).wait_recv()
            k_x(slot, xl, 2, to_xr).start()

        def relay_dn():
            slot = lax.rem(z + e, Z)
            k_x(slot, xr, 1, to_xl).wait_recv()
            k_x(slot, xr, 2, to_xl).start()

        pl.when(e <= HALF)(relay_up)
        pl.when(jnp.logical_and(e >= 1, e <= HALF - 1))(relay_dn)

        w_step(d + W_AHEAD)

        pl.when(d == 1)(make_q)
        pl.when(d == 2)(place_q)
        pl.when(d == HALF + 1)(conv_gates)

        g = d - 2
        last = g == HALF
        slot_a = lax.rem(z - g + Z, Z)
        slot_b = jnp.where(last, z, lax.rem(z + g, Z))

        def attend():
            k_x(slot_a, xr, 1, to_xl).wait_recv()
            k_x(slot_a, xo, 2, to_xr).wait_recv()

            def up_kind():
                k_x(slot_b, xr, 1, to_xl).wait_recv()

            def dn_kind():
                k_x(slot_b, xl, 0, to_xr).wait_recv()

            pl.when(last)(up_kind)
            pl.when(jnp.logical_not(last))(dn_kind)
            k_x(slot_b, xo, 2, to_xr).wait_recv()
            chunk(slot_a, slot_b)

        pl.when(g >= 1)(attend)
        return 0

    lax.fori_loop(1, HALF + 3, step, 0)

    for i in range(H):
        p, e = divmod(i, 2)
        theirs = slice(e * 2 * T + T, (e + 1) * 2 * T)
        o_send[i * VALUE : (i + 1) * VALUE, :] = o_acc[i][:, T:]
        o_send[H * VALUE + i : H * VALUE + i + 1, :] = m_acc[p][:, theirs]
        o_send[H * VALUE + H + i : H * VALUE + H + i + 1, :] = l_acc[p][:, theirs]
    o_exchange = remote(o_send, o_recv, o_s.at[0], o_r.at[0], partner)
    o_exchange.start()

    halo_copy(0, to_next).wait_recv()
    halo_copy(1, to_prev).wait_recv()
    g = gated[...]
    row = lax.broadcasted_iota(jnp.int32, g.shape, 0)
    before = jnp.where(sp == 0, 0.0, halo[0, 7:8, :])
    after = jnp.where(sp == SP - 1, 0.0, halo[1, 0:1, :])
    g_before = jnp.where(row == 0, before, pltpu.roll(g, 1, 0))
    g_after = jnp.where(row == T - 1, after, pltpu.roll(g, T - 1, 0))
    taps = conv_kernel[...].astype(F32)
    conv = g_before * taps[0:1] + g * taps[1:2] + g_after * taps[2:3]
    y_conv = (yconv[...] * conv).astype(BF16)

    o_exchange.wait_recv()
    parts = []
    for i in range(H):
        p, e = divmod(i, 2)
        ours = slice(e * 2 * T, e * 2 * T + T)
        m1 = m_acc[p][:, ours]
        m2 = o_recv[H * VALUE + i : H * VALUE + i + 1, :]
        top = jnp.maximum(m1, m2)
        a1, a2 = jnp.exp2(m1 - top), jnp.exp2(m2 - top)
        total = a1 * l_acc[p][:, ours] + a2 * o_recv[H * VALUE + H + i : H * VALUE + H + i + 1, :]
        summed = a1 * o_acc[i][:, :T] + a2 * o_recv[i * VALUE : (i + 1) * VALUE, :]
        parts.append(summed / total)
    y_attn = jnp.transpose(jnp.concatenate(parts, axis=0)).astype(BF16)
    y = jnp.concatenate([y_conv, y_attn], axis=1)
    for cp in out_cp:
        cp.wait()
    for rel, dev in ((2, to_xo), (1, to_xr), (3, to_xl), (0, None)):
        dest = lax.rem(x + rel, X)
        cols = pl.ds(pl.multiple_of(dest * DX, DX), DX)
        rs_send[rel] = dot_f32(y, wout[:, cols]).astype(BF16)
        if dev is not None:
            remote(rs_send.at[rel], rs_recv.at[rel - 1], r_s.at[rel - 1], r_r.at[rel - 1], dev).start()
    total = rs_send[0].astype(F32)
    r_copies = [
        remote(rs_send.at[rel], rs_recv.at[rel - 1], r_s.at[rel - 1], r_r.at[rel - 1], dev)
        for rel, dev in ((1, to_xr), (3, to_xl), (2, to_xo))
    ]
    for rel, cp in zip((1, 3, 2), r_copies):
        cp.wait_recv()
        total += rs_recv[rel - 1].astype(F32)
    out[...] = total.astype(BF16)

    for cp in tok_sends + [tok_copy(4, xl, lo, to_xr, False), tok_copy(5, xr, hi, to_xl, False)]:
        cp.wait_send()
    for cp in q_sends + [q_exchange, halo_copy(0, to_next), halo_copy(1, to_prev), o_exchange] + r_copies:
        cp.wait_send()

    def sent(d, _):
        k_z(z, d, 0, to_up).wait_send()
        w_z(z, d, 0, to_up).wait_send()

        def back():
            k_z(z, d, 1, to_dn).wait_send()
            w_z(z, d, 1, to_dn).wait_send()

        pl.when(d < HALF - 1)(back)
        return 0

    lax.fori_loop(0, HALF, sent, 0)

    def sent_slots(s, _):
        w_p(s, c).wait_send()
        for kind, dev in ((0, to_xr), (1, to_xl), (2, to_xr)):
            k_x(s, x, kind, dev).wait_send()
        return 0

    lax.fori_loop(0, Z, sent_slots, 0)


def solution(mesh):
    SP, X = mesh.shape["sp"], mesh.shape["tp"]

    def per_device(
        tokens, mix_gain, wv, wo, wi, conv_kernel, wqd, wkvd, wrk, q_gain, kv_gain,
        wqn, wqr, wkn, wval, woc, woa,
    ):
        T, DX = tokens.shape
        D = DX * X
        Z = SP // 2
        R, CC = wv.shape
        H = wqn.shape[1] // NOPE
        nk, nq = wkvd.shape[1], wqd.shape[1]
        RX = ROPE // X
        anyspace = pl.BlockSpec(memory_space=pl.ANY)
        vmem = pl.BlockSpec(memory_space=pltpu.VMEM)
        V = pltpu.VMEM
        DMA = pltpu.SemaphoreType.DMA
        scratch = [
            V((3, Z, 2, R, CC), BF16),
            V((X, T, DX), BF16),
            V((T, D), BF16),
            V(wqd.shape, BF16), V(wkvd.shape, BF16), V(wrk.shape, BF16),
            V((D, nq + 128), BF16),
            V(wqn.shape, BF16), V(wqr.shape, BF16), V(wkn.shape, BF16), V(wval.shape, BF16),
            V((wval.shape[1], wval.shape[0]), BF16),
            V((woc.shape[0] + woa.shape[0], woc.shape[1]), BF16),
            V((X, nq, T), BF16),
            V((H * (NOPE + ROPE), T), BF16), V((H * (NOPE + ROPE), T), BF16),
            V((H // 2, 256, 4 * T), BF16),
            V((Z, X, nk + 2 * RX, T), BF16),
            V((ROPE, T), F32), V((2, ROPE, T), F32),
            V((nq * X, 128), F32), V((nk * X, 128), F32),
            V((T, 128), F32),
            V((H, VALUE, 2 * T), F32), V((H // 2, 1, 4 * T), F32), V((H // 2, 1, 4 * T), F32),
            V((H * VALUE + 2 * H, T), F32), V((H * VALUE + 2 * H, T), F32),
            V((T, CC), F32), V((2, 8, CC), F32), V((T, CC), F32),
            V((X, T, DX), BF16), V((X - 1, T, DX), BF16),
            DMA((13,)),
            DMA((6,)), DMA((6,)),
            DMA((3,)), DMA((3,)), DMA((1,)), DMA((1,)),
            DMA((2, Z // 2)), DMA((Z,)), DMA((Z, 3)), DMA((Z, 3)),
            DMA((2, Z // 2)), DMA((Z,)), DMA((Z,)), DMA((Z,)),
            DMA((1,)), DMA((1,)), DMA((2,)), DMA((2,)), DMA((3,)), DMA((3,)),
        ]
        return pl.pallas_call(
            functools.partial(kernel, SP, X),
            out_shape=jax.ShapeDtypeStruct((T, DX), BF16),
            in_specs=[anyspace, vmem, anyspace, anyspace, anyspace, vmem, anyspace, anyspace, anyspace,
                      vmem, vmem] + [anyspace] * 6,
            out_specs=vmem,
            scratch_shapes=scratch,
            compiler_params=pltpu.CompilerParams(
                collective_id=0, has_side_effects=True, vmem_limit_bytes=56 * 1024 * 1024
            ),
        )(
            tokens, mix_gain.reshape(1, -1), wv, wo, wi, conv_kernel, wqd, wkvd, wrk,
            q_gain.reshape(1, -1), kv_gain.reshape(1, -1), wqn, wqr, wkn, wval, woc, woa,
        )

    placed = (
        P(("grp", "sp"), "tp"),
        P(),
        P("sp", "tp"),
        P("sp", "tp"),
        P("sp", "tp"),
        P(None, "tp"),
        P(None, "tp"),
        P(None, "tp"),
        P(),
        P(),
        P(),
        P(None, "tp"),
        P(None, "tp"),
        P(None, "tp"),
        P(None, "tp"),
        P("tp", None),
        P("tp", None),
    )
    return jax.shard_map(
        per_device, mesh=mesh, in_specs=placed, out_specs=P(("grp", "sp"), "tp"), check_vma=False
    )
```

time: 388 us -> 139 us (0.36)
  waiting for transfers between devices: 269 us -> 0 us
  Pallas kernels: 0 us -> 131 us
  matrix products: 49.2 us -> 0 us
  blocking collectives: 22.1 us -> 0 us
  between operations: 13.9 us -> 0.01 us
  starting transfers between devices: 9.56 us -> 0 us
  local copies, waits for them, and re-layouts: 15.4 us -> 7.64 us
  other arithmetic: 6.97 us -> 0 us
    all_gather x2 -> x0, waiting for transfers between devices: 259 us -> none  [sent_together(): lax.all_gather(both, axis, axis=dim, tiled=True)]
    pallas_call x0 -> x1, Pallas kernels: none -> 131 us  [per_device(): pl.pallas_call(functools.partial(kernel, SP, X), out_shape=jax.ShapeDtype...]
    dot_general x49 -> x0, matrix products: 49.2 us -> none  [the longest x8 11.1 us: one_block(): jnp.dot(latent_block, w_k_nope, preferred_element_type=f32).astype(bf16)]
    all_to_all x1 -> x0, blocking collectives: 12.8 us -> none  [summed_on_arrival(): lax.all_to_all(tiles, axis, split_axis=0, concat_axis=0, tiled=True)]
    all_gather x1 -> x0, blocking collectives: 9.29 us -> none  [one_gather(): lines, at, done = (lax.all_gather(vector, axis), 0, [])]
    all_to_all x1 -> x0, waiting for transfers between devices: 6.8 us -> none  [from_everyone(): return lax.all_to_all(copies, axis, split_axis=0, concat_axis=0, tiled=True)]
    all_to_all x1 -> x0, starting transfers between devices: 5.12 us -> none  [from_everyone(): return lax.all_to_all(copies, axis, split_axis=0, concat_axis=0, tiled=True)]
    split x3 -> x0, local copies, waits for them, and re-layouts: 4.65 us -> none  [sent_together(): jnp.split(lax.all_gather(both, axis, axis=dim, tiled=True), ends, axis=al...]
  transfers between devices with their start and end apart: 5 -> 0, of which waited for: 4 -> 0; matrix products, arithmetic and copies ran while one was open for 3% -> 0% of each run, Pallas kernels for 0% -> 0%
where the time goes in v1:
time: 139 us
  Pallas kernels  131 us (94%)
  local copies, waits for them, and re-layouts  7.64 us (5%)
    pallas_call x1, Pallas kernels, per_device(): pl.pallas_call(functools.partial(kernel, SP, X), out_shape=jax.ShapeDtype...  131 us
    unnamed x7, local copies, waits for them, and re-layouts  4.55 us

profile of v1, /device:TPU:33, one launch (start us, length us, event | category | flops | bytes accessed | tf_op | source)
XLA Modules:
  0.0 139.0 jit_solution(1249056820576325053)
XLA Ops:
  0.0 0.0 copy-start.1
  0.0 1.2 reshape.11.kv_gain
  1.2 1.2 reshape.10.q_gain
  2.5 0.0 copy-done.1
  2.5 0.6 reshape.9.mix_gain
  3.1 0.0 copy-start
  3.1 2.0 %copy.18.wkvd = bf16[2048,64]{1,0:T(8,128)(2,1)} copy(bf16[2048,64]{0,1:T(8,128)(2,1)} %param.24) | data formatting | bytes 524288 | tf_op args[7]
  5.1 0.0 copy-done
  5.1 1.0 copy.19.wrk
  6.1 131.4 %shard_map.163 = bf16[128,512]{1,0:T(8,128)(2,1)} custom-call(bf16[128,512]{1,0:T(8,128)(2,1)} %tokens.1, bf16[1,2048]{1,0:T(2,128)(2,1)} %reshape.9.mix_gain, bf16[32,256]{1,0:T(8,128)(2,1)} %wv.1, bf16[32,256]{1,0:T(8,128)(2,1)} %wo.1, bf16[32,256]{1,0:T(8,128)(2,1)} %wi.1, bf16[3,256]{1,0:T(4,128)(2,1)} %conv_kernel.1, bf16[2048,128]{1,0:T(8,128)(2,1)} %wqd.1, ...), custom_call_target="tpu_custom_call" | custom-call | tf_op jit(solution)/shard_map/pallas_call | solution.py:484
  137.5 1.6 %copy.21 = bf16[128,512]{1,0:T(8,128)(2,1)} copy(bf16[128,512]{1,0:T(8,128)(2,1)} %shard_map.163) | data formatting | bytes 262144
Async XLA Ops:
  0.0 2.5 %copy-start.1 = (bf16[2048]{0:T(1024)(128)(2,1)S(1)}, bf16[2048]{0:T(1024)(128)(2,1)}, u32[]{:S(2)}) copy-start(bf16[2048]{0:T(1024)(128)(2,1)} %param.18) | copy-start | bytes 12292
  3.1 2.0 %copy-start = (bf16[2048,32]{0,1:T(8,128)(2,1)S(1)}, bf16[2048,32]{0,1:T(8,128)(2,1)}, u32[]{:S(2)}) copy-start(bf16[2048,32]{0,1:T(8,128)(2,1)} %param.25) | copy-start | bytes 393220

commit v2 on v1

--- a/solution.py
+++ b/solution.py
@@ -17,7 +17,9 @@
 MESH = pl.DeviceIdType.MESH
 F32 = jnp.float32
 BF16 = jnp.bfloat16
-W_AHEAD = 3
+STRIDE = 3
+W_FIRST = 3
+W_EACH = 2
 
 
 def dot_f32(a, b, contract=((1,), (0,))):
@@ -29,14 +31,16 @@
     tokens, mix_gain, wv, wo, wi, conv_kernel, wqd, wkvd, wrk, q_gain, kv_gain,
     wqn, wqr, wkn, wval, woc, woa,
     out,
-    wbuf, tok, scaled, wqd_v, wkvd_v, wrk_v, wd, wqn_v, wqr_v, wkn_v, wval_v, wval_t, wout,
+    wbuf, tok, scaled, wqd_v, wd_t, wqn_v, wqr_v, wkn_v, wval_v, wval_t, wout,
     qbuf, qmine, qpart, qz, kvbuf, rope_scr, cs_scr, qg_col, kvg_col, rs_scr,
     o_acc, m_acc, l_acc, o_send, o_recv, gated, halo, yconv, rs_send, rs_recv,
-    loc, tk_s, tk_r, q_s, q_r, qp_s, qp_r, kz_s, kz_r, kx_s, kx_r, wz_s, wz_r, wp_s, wp_r,
+    loc, tk_s, tk_r, q_s, q_r, qp_s, qp_r, kf_s, kn_s, kz_r, kx_s, kx_r, wz_s, wz_r, wp_s, wp_r, wq_s, wq_r,
     o_s, o_r, h_s, h_r, r_s, r_r,
 ):
     Z = SP // 2
     HALF = Z // 2
+    K = (HALF - 1) // STRIDE
+    assert HALF == STRIDE * K + 1
     T = tokens.shape[0]
     DX = tokens.shape[1]
     D = DX * X
@@ -45,13 +49,14 @@
     x = lax.axis_index("tp")
     z = lax.div(sp, 2)
     c = lax.rem(sp, 2)
-    up = lax.rem(z + 1, Z)
-    dn = lax.rem(z + Z - 1, Z)
+    def core_at(step):
+        return {"sp": lax.rem(z + step + Z, Z) * 2 + c}
+
     xr = lax.rem(x + 1, X)
     xl = lax.rem(x + X - 1, X)
     xo = lax.rem(x + 2, X)
-    to_up = {"sp": up * 2 + c}
-    to_dn = {"sp": dn * 2 + c}
+    to_up, to_dn = core_at(1), core_at(-1)
+    far_up, far_dn = core_at(STRIDE), core_at(-STRIDE)
     partner = {"sp": z * 2 + 1 - c}
     to_xr, to_xl, to_xo = {"tp": xr}, {"tp": xl}, {"tp": xo}
     prev_sp = lax.rem(sp + SP - 1, SP)
@@ -72,15 +77,16 @@
 
     conv_cp = [bring(w, wbuf.at[i, z, c]) for i, w in enumerate((wv, wo, wi))]
     tok_cp = bring(tokens, tok.at[x])
-    down_cp = [bring(wqd, wqd_v), bring(wkvd, wkvd_v), bring(wrk, wrk_v)]
+    nk, nr = wkvd.shape[0], wrk.shape[0]
+    down_cp = [bring(wqd, wqd_v), bring(wkvd, wd_t.at[pl.ds(0, nk)]), bring(wrk, wd_t.at[pl.ds(nk, nr)])]
     up_cp = [bring(wqn, wqn_v), bring(wqr, wqr_v), bring(wkn, wkn_v), bring(wval, wval_v)]
     NC = woc.shape[0]
     out_cp = [bring(woc, wout.at[pl.ds(0, NC)]), bring(woa, wout.at[pl.ds(NC, woa.shape[0])])]
 
     barrier = pltpu.get_barrier_semaphore()
-    for dev in (to_up, to_dn, partner, to_xr, to_xl, to_xo, other_chip):
+    for dev in (to_up, to_dn, far_up, far_dn, partner, to_xr, to_xl, to_xo, other_chip):
         pl.semaphore_signal(barrier, inc=1, device_id=dev, device_id_type=MESH)
-    pl.semaphore_wait(barrier, 7)
+    pl.semaphore_wait(barrier, 9)
 
     h = T // 2
     lo, hi = pl.ds(0, h), pl.ds(h, h)
@@ -96,48 +102,46 @@
     for cp in tok_sends:
         cp.start()
 
-    def w_z(slot, d, way, dev):
-        return remote(wbuf.at[:, slot, c], wbuf.at[:, slot, c], wz_s.at[way, d], wz_r.at[slot], dev)
-
-    def w_p(slot, core):
-        return remote(wbuf.at[:, slot, core], wbuf.at[:, slot, core], wp_s.at[slot], wp_r.at[slot], partner)
+    def w_z(slot, d, way, core, dev):
+        piece = wbuf.at[:, slot, core]
+        return remote(piece, piece, wz_s.at[way, d, core], wz_r.at[slot, core], dev)
+
+    def w_p(slot):
+        return remote(wbuf.at[:, slot], wbuf.at[:, slot], wp_s.at[slot], wp_r.at[slot], partner)
+
+    def w_own(core):
+        return remote(wbuf.at[:, z, core], wbuf.at[:, z, core], wq_s.at[0], wq_r.at[0], partner)
 
     for cp in conv_cp:
         cp.wait()
-    w_z(z, 0, 0, to_up).start()
-    w_z(z, 0, 1, to_dn).start()
-    w_p(z, c).start()
-
-    def when(cond, fn):
-        if isinstance(cond, bool):
-            if cond:
-                fn()
-        else:
-            pl.when(cond)(fn)
+    w_own(c).start()
+
+    def w_begin(core):
+        w_z(z, 0, 0, core, to_up).start()
+        w_z(z, 0, 1, core, to_dn).start()
+
+    pl.when(c == 1)(lambda: w_begin(1))
+
+    def w_in(k, way):
+        slot = lax.rem(z - k + Z, Z) if way == 0 else lax.rem(z + k, Z)
+        dev = to_up if way == 0 else to_dn
+        end = HALF if way == 0 else HALF - 1
+        for core in (1, 0):
+            w_z(slot, k, way, core, dev).wait_recv()
+            pl.when(k < end)(lambda core=core: w_z(slot, k, way, core, dev).start())
+        w_p(slot).start()
 
     def w_step(k):
-        def go_up():
-            slot = lax.rem(z - k + Z, Z)
-            w_z(slot, k, 0, to_up).wait_recv()
-            when(k < HALF, lambda: w_z(slot, k, 0, to_up).start())
-            w_p(slot, c).start()
-
-        def go_dn():
-            slot = lax.rem(z + k, Z)
-            w_z(slot, k, 1, to_dn).wait_recv()
-            when(k < HALF - 1, lambda: w_z(slot, k, 1, to_dn).start())
-            w_p(slot, c).start()
-
-        when(k <= HALF, go_up)
-        when(k <= HALF - 1, go_dn)
-
-    for cp in down_cp:
-        cp.wait()
-    wd[:, : wqd.shape[1]] = wqd_v[...]
-    nk, nr = wkvd.shape[1], wrk.shape[1]
-    wd[:, wqd.shape[1] :] = jnp.concatenate(
-        [wkvd_v[...], wrk_v[...], jnp.zeros((D, 128 - nk - nr), BF16)], axis=1
-    )
+        pl.when(jnp.logical_and(c == 1, k <= HALF))(lambda: w_in(k, 0))
+        pl.when(jnp.logical_and(c == 1, k <= HALF - 1))(lambda: w_in(k, 1))
+
+    def w_steps(first, count):
+        def one(i, _):
+            w_step(first + i)
+            return 0
+        lax.fori_loop(0, count, one, 0)
+
+    wd_t[nk + nr :, :] = jnp.zeros((wd_t.shape[0] - nk - nr, D), BF16)
     rows16 = lax.broadcasted_iota(jnp.int32, (ROPE, T), 0)
     freq = jnp.where(rows16 >= ROPE // 2, rows16 - ROPE // 2, rows16).astype(F32) * 2.0
     inverse = jnp.exp(freq * (-math.log(THETA) / ROPE))
@@ -154,28 +158,34 @@
         cp.wait()
     wval_t[...] = jnp.transpose(wval_v[...].astype(F32)).astype(BF16)
 
+    w_own(1 - c).wait_recv()
+    pl.when(c == 1)(lambda: w_begin(0))
     tok_copy(0, xl, lo, to_xr, False).wait_recv()
     tok_copy(4, xl, lo, to_xr, False).start()
     tok_copy(2, xr, hi, to_xl, False).wait_recv()
     tok_copy(5, xr, hi, to_xl, False).start()
     tok_copy(1, xl, hi, to_xr, False).wait_recv()
     tok_copy(3, xr, lo, to_xl, False).wait_recv()
-    w_step(1)
+    w_steps(1, 1)
     tok_copy(4, xo, lo, to_xr, False).wait_recv()
     tok_copy(5, xo, hi, to_xl, False).wait_recv()
     tok_cp.wait()
 
-    down = jnp.zeros((T, wd.shape[1]), F32)
+    for cp in down_cp:
+        cp.wait()
+    down_q = jnp.zeros((T, wqd.shape[1]), F32)
+    down_k = jnp.zeros((T, wd_t.shape[0]), F32)
     squares = jnp.zeros((T, 1), F32)
     for j in range(X):
         t = tok[j].astype(F32)
         s = (t * mix_gain[:, j * DX : (j + 1) * DX].astype(F32)).astype(BF16)
         scaled[:, j * DX : (j + 1) * DX] = s
         squares += jnp.sum(t * t, axis=1, keepdims=True)
-        down += dot_f32(s, wd[j * DX : (j + 1) * DX, :])
+        down_q += dot_f32(s, wqd_v[j * DX : (j + 1) * DX, :])
+        down_k += dot_f32(s, wd_t[:, j * DX : (j + 1) * DX], ((1,), (1,)))
     row_scale = lax.rsqrt(squares / D + EPS)
     rs_scr[...] = jnp.broadcast_to(row_scale, rs_scr.shape)
-    down_t = jnp.transpose(down * row_scale)
+    down_t = jnp.transpose(jnp.concatenate([down_q, down_k], axis=1) * row_scale)
     nq = wqd.shape[1]
     kv_rows = pl.ds(0, nk)
     kvbuf[z, x, kv_rows, :] = down_t[nq : nq + nk].astype(BF16)
@@ -190,14 +200,21 @@
     mine = rope_scr[pl.ds(pl.multiple_of(x * RX, RX), RX), :]
     kvbuf[z, x, pl.ds(nk, 2 * RX), :] = jnp.concatenate([mine, jnp.zeros((RX, T), F32)], axis=0).astype(BF16)
 
-    def k_z(slot, d, way, dev):
-        return remote(kvbuf.at[slot, x], kvbuf.at[slot, x], kz_s.at[way, d], kz_r.at[slot], dev)
+    def k_far(slot, j, way):
+        piece = kvbuf.at[slot, x]
+        return remote(piece, piece, kf_s.at[way, j], kz_r.at[slot], far_dn if way else far_up)
+
+    def k_near(slot, way):
+        piece = kvbuf.at[slot, x]
+        return remote(piece, piece, kn_s.at[slot, way], kz_r.at[slot], to_dn if way else to_up)
 
     def k_x(slot, piece, kind, dev):
         return remote(kvbuf.at[slot, piece], kvbuf.at[slot, piece], kx_s.at[slot, kind], kx_r.at[slot, kind], dev)
 
-    k_z(z, 0, 0, to_up).start()
-    k_z(z, 0, 1, to_dn).start()
+    k_far(z, 0, 0).start()
+    k_far(z, 0, 1).start()
+    k_near(z, 0).start()
+    k_near(z, 1).start()
     k_x(z, x, 0, to_xr).start()
     k_x(z, x, 1, to_xl).start()
 
@@ -209,9 +226,7 @@
     q_sends = [q_copy(2, x, to_xo), q_copy(0, x, to_xr), q_copy(1, x, to_xl)]
     for cp in q_sends:
         cp.start()
-    for k in range(2, W_AHEAD + 1):
-        if k <= HALF:
-            w_step(k)
+    w_steps(2, W_FIRST - 1)
 
     factor = (NOPE + ROPE) ** (-0.5) * LOG2E
     q_exchange = remote(qmine, qpart, qp_s.at[0], qp_r.at[0], partner)
@@ -278,10 +293,15 @@
     to_next, to_prev = {"sp": next_sp}, {"sp": prev_sp}
 
     def conv_gates():
-        def got(s, _):
-            w_p(s, 1 - c).wait_recv()
+        def got(i, _):
+            w_p(lax.rem(z + i, Z)).wait_recv()
             return 0
-        lax.fori_loop(0, Z, got, 0)
+
+        def all_in():
+            lax.fori_loop(1, Z, got, 0)
+
+        pl.when(c == 0)(all_in)
+
         def project(i):
             w = wbuf[i].reshape(D, wbuf.shape[-1])
             return (dot_f32(scaled[...], w) * rs_scr[:, 0:1]).astype(BF16).astype(F32)
@@ -292,69 +312,99 @@
         halo_copy(1, to_prev).start()
         yconv[...] = project(1)
 
-    def step(d, _):
-        def up_in():
-            slot = lax.rem(z - d + Z, Z)
-            k_z(slot, d, 0, to_up).wait_recv()
-            pl.when(d < HALF)(lambda: k_z(slot, d, 0, to_up).start())
-            k_x(slot, x, 0, to_xr).start()
-            k_x(slot, x, 1, to_xl).start()
-
-        def dn_in():
-            slot = lax.rem(z + d, Z)
-            k_z(slot, d, 1, to_dn).wait_recv()
-            pl.when(d < HALF - 1)(lambda: k_z(slot, d, 1, to_dn).start())
-            k_x(slot, x, 0, to_xr).start()
-            k_x(slot, x, 1, to_xl).start()
-
-        pl.when(d <= HALF)(up_in)
-        pl.when(d <= HALF - 1)(dn_in)
-
-        e = d - 1
-
-        def relay_up():
-            slot = lax.rem(z - e + Z, Z)
-            k_x(slot, xl, 0, to_xr).wait_recv()
-            k_x(slot, xl, 2, to_xr).start()
-
-        def relay_dn():
-            slot = lax.rem(z + e, Z)
-            k_x(slot, xr, 1, to_xl).wait_recv()
-            k_x(slot, xr, 2, to_xl).start()
-
-        pl.when(e <= HALF)(relay_up)
-        pl.when(jnp.logical_and(e >= 1, e <= HALF - 1))(relay_dn)
-
-        w_step(d + W_AHEAD)
-
-        pl.when(d == 1)(make_q)
-        pl.when(d == 2)(place_q)
-        pl.when(d == HALF + 1)(conv_gates)
-
-        g = d - 2
-        last = g == HALF
-        slot_a = lax.rem(z - g + Z, Z)
-        slot_b = jnp.where(last, z, lax.rem(z + g, Z))
-
-        def attend():
-            k_x(slot_a, xr, 1, to_xl).wait_recv()
-            k_x(slot_a, xo, 2, to_xr).wait_recv()
-
-            def up_kind():
-                k_x(slot_b, xr, 1, to_xl).wait_recv()
-
-            def dn_kind():
-                k_x(slot_b, xl, 0, to_xr).wait_recv()
-
-            pl.when(last)(up_kind)
-            pl.when(jnp.logical_not(last))(dn_kind)
-            k_x(slot_b, xo, 2, to_xr).wait_recv()
-            chunk(slot_a, slot_b)
-
-        pl.when(g >= 1)(attend)
+    def at(offset):
+        return lax.rem(z + offset + 2 * Z, Z)
+
+    def spread(slot):
+        k_x(slot, x, 0, to_xr).start()
+        k_x(slot, x, 1, to_xl).start()
+
+    def stop(j, way):
+        slot = at(STRIDE * j if way else -STRIDE * j)
+        k_near(slot, 0).wait_recv()
+        pl.when(j < K)(lambda: k_far(slot, j, way).start())
+        if way == 0:
+            k_near(slot, 0).start()
+            k_near(slot, 1).start()
+        else:
+            k_near(slot, 0).start()
+            pl.when(j < K)(lambda: k_near(slot, 1).start())
+        spread(slot)
+
+    def leaf(slot):
+        k_near(slot, 0).wait_recv()
+        spread(slot)
+
+    def relay_up(slot):
+        k_x(slot, xl, 0, to_xr).wait_recv()
+        k_x(slot, xl, 2, to_xr).start()
+
+    def relay_dn(slot):
+        k_x(slot, xr, 1, to_xl).wait_recv()
+        k_x(slot, xr, 2, to_xl).start()
+
+    def leaves(j, fn_up, fn_dn):
+        def inner():
+            fn_up(at(-STRIDE * j + 1))
+            fn_dn(at(STRIDE * j - 1))
+
+        fn_up(at(-STRIDE * j - 1))
+        pl.when(j < K)(lambda: fn_dn(at(STRIDE * j + 1)))
+        pl.when(j >= 1)(inner)
+
+    def got_up(slot):
+        k_x(slot, xr, 1, to_xl).wait_recv()
+        k_x(slot, xo, 2, to_xr).wait_recv()
+
+    def got_dn(slot):
+        k_x(slot, xl, 0, to_xr).wait_recv()
+        k_x(slot, xo, 2, to_xl).wait_recv()
+
+    def pair(j, r):
+        off = STRIDE * j + jnp.where(r == 0, 0, jnp.where(r == 1, -1, 1))
+        own = off == HALF
+        slot_a = at(-off)
+        slot_b = jnp.where(own, z, at(off))
+        got_up(slot_a)
+        pl.when(own)(lambda: got_up(slot_b))
+        pl.when(jnp.logical_not(own))(lambda: got_dn(slot_b))
+        chunk(slot_a, slot_b)
+
+    def step(i, _):
+        def stops_in():
+            stop(i, 0)
+            stop(i, 1)
+
+        pl.when(i <= K)(stops_in)
+        pl.when(i - 1 <= K)(lambda: leaves(i - 1, leaf, leaf))
+
+        def relay_stops():
+            relay_up(at(-STRIDE * (i - 1)))
+            pl.when(i - 1 >= 1)(lambda: relay_dn(at(STRIDE * (i - 1))))
+
+        pl.when(i - 1 <= K)(relay_stops)
+        pl.when(jnp.logical_and(i - 2 >= 0, i - 2 <= K))(lambda: leaves(i - 2, relay_up, relay_dn))
+
+        pl.when(i <= K + 1)(lambda: w_steps(W_FIRST + 1 + W_EACH * (i - 1), W_EACH))
+
+        pl.when(i == 1)(make_q)
+        pl.when(i == 2)(place_q)
+        pl.when(i == K + 1)(w_rest)
+
+        def one(r, _):
+            j = jnp.where(r == 0, i - 2, i - 3)
+            here = jnp.logical_and(j >= jnp.where(r == 2, 0, 1), j <= K)
+            pl.when(here)(lambda: pair(j, r))
+            return 0
+
+        lax.fori_loop(0, 3, one, 0)
         return 0
 
-    lax.fori_loop(1, HALF + 3, step, 0)
+    def w_rest():
+        w_steps(W_FIRST + 1 + W_EACH * (K + 1), HALF - W_FIRST - W_EACH * (K + 1))
+        conv_gates()
+
+    lax.fori_loop(1, K + 4, step, 0)
 
     for i in range(H):
         p, e = divmod(i, 2)
@@ -414,21 +464,45 @@
     for cp in q_sends + [q_exchange, halo_copy(0, to_next), halo_copy(1, to_prev), o_exchange] + r_copies:
         cp.wait_send()
 
-    def sent(d, _):
-        k_z(z, d, 0, to_up).wait_send()
-        w_z(z, d, 0, to_up).wait_send()
+    w_own(c).wait_send()
+
+    def w_sent(d, _):
+        for core in (0, 1):
+            w_z(z, d, 0, core, to_up).wait_send()
 
         def back():
-            k_z(z, d, 1, to_dn).wait_send()
-            w_z(z, d, 1, to_dn).wait_send()
+            for core in (0, 1):
+                w_z(z, d, 1, core, to_dn).wait_send()
 
         pl.when(d < HALF - 1)(back)
         return 0
 
-    lax.fori_loop(0, HALF, sent, 0)
+    def w_handed(i, _):
+        w_p(lax.rem(z + i, Z)).wait_send()
+        return 0
+
+    def w_all():
+        lax.fori_loop(0, HALF, w_sent, 0)
+        lax.fori_loop(1, Z, w_handed, 0)
+
+    pl.when(c == 1)(w_all)
+
+    def k_sent(j, _):
+        for way in (0, 1):
+            pl.when(j < K)(lambda way=way: k_far(z, j, way).wait_send())
+        k_near(at(-STRIDE * j), 0).wait_send()
+        k_near(at(-STRIDE * j), 1).wait_send()
+
+        def back():
+            k_near(at(STRIDE * j), 0).wait_send()
+            pl.when(j < K)(lambda: k_near(at(STRIDE * j), 1).wait_send())
+
+        pl.when(j >= 1)(back)
+        return 0
+
+    lax.fori_loop(0, K + 1, k_sent, 0)
 
     def sent_slots(s, _):
-        w_p(s, c).wait_send()
         for kind, dev in ((0, to_xr), (1, to_xl), (2, to_xr)):
             k_x(s, x, kind, dev).wait_send()
         return 0
@@ -449,6 +523,7 @@
         R, CC = wv.shape
         H = wqn.shape[1] // NOPE
         nk, nq = wkvd.shape[1], wqd.shape[1]
+        K = (Z // 2 - 1) // STRIDE
         RX = ROPE // X
         anyspace = pl.BlockSpec(memory_space=pl.ANY)
         vmem = pl.BlockSpec(memory_space=pltpu.VMEM)
@@ -458,8 +533,8 @@
             V((3, Z, 2, R, CC), BF16),
             V((X, T, DX), BF16),
             V((T, D), BF16),
-            V(wqd.shape, BF16), V(wkvd.shape, BF16), V(wrk.shape, BF16),
-            V((D, nq + 128), BF16),
+            V(wqd.shape, BF16),
+            V((128, D), BF16),
             V(wqn.shape, BF16), V(wqr.shape, BF16), V(wkn.shape, BF16), V(wval.shape, BF16),
             V((wval.shape[1], wval.shape[0]), BF16),
             V((woc.shape[0] + woa.shape[0], woc.shape[1]), BF16),
@@ -477,8 +552,8 @@
             DMA((13,)),
             DMA((6,)), DMA((6,)),
             DMA((3,)), DMA((3,)), DMA((1,)), DMA((1,)),
-            DMA((2, Z // 2)), DMA((Z,)), DMA((Z, 3)), DMA((Z, 3)),
-            DMA((2, Z // 2)), DMA((Z,)), DMA((Z,)), DMA((Z,)),
+            DMA((2, K)), DMA((Z, 2)), DMA((Z,)), DMA((Z, 3)), DMA((Z, 3)),
+            DMA((2, Z // 2, 2)), DMA((Z, 2)), DMA((Z,)), DMA((Z,)), DMA((1,)), DMA((1,)),
             DMA((1,)), DMA((1,)), DMA((2,)), DMA((2,)), DMA((3,)), DMA((3,)),
         ]
         return pl.pallas_call(
@@ -492,7 +567,7 @@
                 collective_id=0, has_side_effects=True, vmem_limit_bytes=56 * 1024 * 1024
             ),
         )(
-            tokens, mix_gain.reshape(1, -1), wv, wo, wi, conv_kernel, wqd, wkvd, wrk,
+            tokens, mix_gain.reshape(1, -1), wv, wo, wi, conv_kernel, wqd, wkvd.T, wrk.T,
             q_gain.reshape(1, -1), kv_gain.reshape(1, -1), wqn, wqr, wkn, wval, woc, woa,
         )
 

time: 139 us -> 130 us (0.935)
  Pallas kernels: 131 us -> 126 us
  local copies, waits for them, and re-layouts: 7.64 us -> 3.97 us
    pallas_call x1, Pallas kernels: 131 us -> 126 us  [per_device(): pl.pallas_call(functools.partial(kernel, SP, X), out_shape=jax.ShapeDtype...]
    unnamed x7 -> x5, local copies, waits for them, and re-layouts: 4.55 us -> 1.58 us
where the time goes in v2:
time: 130 us
  Pallas kernels  126 us (97%)
  local copies, waits for them, and re-layouts  3.97 us (3%)
    pallas_call x1, Pallas kernels, per_device(): pl.pallas_call(functools.partial(kernel, SP, X), out_shape=jax.ShapeDtype...  126 us

profile of v2, /device:TPU:33, one launch (start us, length us, event | category | flops | bytes accessed | tf_op | source)
XLA Modules:
  0.0 129.9 jit_solution(5589035716034829495)
XLA Ops:
  0.0 0.0 copy-start
  0.0 0.0 copy-start.1
  0.0 1.2 reshape.11.kv_gain
  1.2 0.0 copy-done.1
  1.2 0.6 reshape.10.q_gain
  1.8 0.0 copy-done
  1.8 0.6 reshape.9.mix_gain
  2.4 125.9 %shard_map.163 = bf16[128,512]{1,0:T(8,128)(2,1)} custom-call(bf16[128,512]{1,0:T(8,128)(2,1)} %tokens.1, bf16[1,2048]{1,0:T(2,128)(2,1)} %reshape.9.mix_gain, bf16[32,256]{1,0:T(8,128)(2,1)} %wv.1, bf16[32,256]{1,0:T(8,128)(2,1)} %wo.1, bf16[32,256]{1,0:T(8,128)(2,1)} %wi.1, bf16[3,256]{1,0:T(4,128)(2,1)} %conv_kernel.1, bf16[2048,128]{1,0:T(8,128)(2,1)} %wqd.1, ...), custom_call_target="tpu_custom_call" | custom-call | tf_op jit(solution)/shard_map/pallas_call | solution.py:559
  128.3 1.6 %copy.19 = bf16[128,512]{1,0:T(8,128)(2,1)} copy(bf16[128,512]{1,0:T(8,128)(2,1)} %shard_map.163) | data formatting | bytes 262144
Async XLA Ops:
  0.0 1.8 %copy-start = (bf16[2048]{0:T(1024)(128)(2,1)S(1)}, bf16[2048]{0:T(1024)(128)(2,1)}, u32[]{:S(2)}) copy-start(bf16[2048]{0:T(1024)(128)(2,1)} %param.18) | copy-start | bytes 12292
  0.0 1.2 copy-start.1

commit v3 on v2

--- a/solution.py
+++ b/solution.py
@@ -32,9 +32,9 @@
     wqn, wqr, wkn, wval, woc, woa,
     out,
     wbuf, tok, scaled, wqd_v, wd_t, wqn_v, wqr_v, wkn_v, wval_v, wval_t, wout,
-    qbuf, qmine, qpart, qz, kvbuf, rope_scr, cs_scr, qg_col, kvg_col, rs_scr,
+    qbuf, qmine, qpart, qz, kvbuf, kv_mine, rope_scr, cs_scr, qg_col, kvg_col, rs_scr,
     o_acc, m_acc, l_acc, o_send, o_recv, gated, halo, yconv, rs_send, rs_recv,
-    loc, tk_s, tk_r, q_s, q_r, qp_s, qp_r, kf_s, kn_s, kz_r, kx_s, kx_r, wz_s, wz_r, wp_s, wp_r, wq_s, wq_r,
+    loc, tk_s, tk_r, q_s, q_r, qp_s, qp_r, kf_s, kn_s, ko_s, ko_r, kh_s, kh_r, kz_r, kx_s, kx_r, wz_s, wz_r, wp_s, wp_r, wq_s, wq_r,
     o_s, o_r, h_s, h_r, r_s, r_r,
 ):
     Z = SP // 2
@@ -187,8 +187,7 @@
     rs_scr[...] = jnp.broadcast_to(row_scale, rs_scr.shape)
     down_t = jnp.transpose(jnp.concatenate([down_q, down_k], axis=1) * row_scale)
     nq = wqd.shape[1]
-    kv_rows = pl.ds(0, nk)
-    kvbuf[z, x, kv_rows, :] = down_t[nq : nq + nk].astype(BF16)
+    kv_mine[:nk, :] = down_t[nq : nq + nk].astype(BF16)
 
     def turned(v, cosine, sine):
         half = ROPE // 2
@@ -198,7 +197,14 @@
     rope_scr[...] = turned(raw, cs_scr[0], cs_scr[1])
     RX = ROPE // X
     mine = rope_scr[pl.ds(pl.multiple_of(x * RX, RX), RX), :]
-    kvbuf[z, x, pl.ds(nk, 2 * RX), :] = jnp.concatenate([mine, jnp.zeros((RX, T), F32)], axis=0).astype(BF16)
+    kv_mine[nk:, :] = jnp.concatenate([mine, jnp.zeros((RX, T), F32)], axis=0).astype(BF16)
+    k_own = remote(kv_mine, kvbuf.at[z, x, 1], ko_s.at[0], ko_r.at[0], partner)
+    pl.when(c == 1)(k_own.start)
+
+    def keep_mine():
+        kvbuf[z, x, 0] = kv_mine[...]
+
+    pl.when(c == 0)(keep_mine)
 
     def k_far(slot, j, way):
         piece = kvbuf.at[slot, x]
@@ -211,12 +217,18 @@
     def k_x(slot, piece, kind, dev):
         return remote(kvbuf.at[slot, piece], kvbuf.at[slot, piece], kx_s.at[slot, kind], kx_r.at[slot, kind], dev)
 
-    k_far(z, 0, 0).start()
-    k_far(z, 0, 1).start()
-    k_near(z, 0).start()
-    k_near(z, 1).start()
-    k_x(z, x, 0, to_xr).start()
-    k_x(z, x, 1, to_xl).start()
+    def k_hand(slot):
+        return remote(kvbuf.at[slot, :, 1], kvbuf.at[slot, :, 1], kh_s.at[slot], kh_r.at[slot], partner)
+
+    def k_begin():
+        k_own.wait_recv()
+        k_far(z, 0, 0).start()
+        k_far(z, 0, 1).start()
+        k_near(z, 0).start()
+        k_near(z, 1).start()
+        k_x(z, x, 0, to_xr).start()
+        k_x(z, x, 1, to_xl).start()
+
 
     qbuf[x] = down_t[:nq].astype(BF16)
 
@@ -226,6 +238,7 @@
     q_sends = [q_copy(2, x, to_xo), q_copy(0, x, to_xr), q_copy(1, x, to_xl)]
     for cp in q_sends:
         cp.start()
+    pl.when(c == 0)(k_begin)
     w_steps(2, W_FIRST - 1)
 
     factor = (NOPE + ROPE) ** (-0.5) * LOG2E
@@ -256,8 +269,8 @@
                 qz[p, 2 * NOPE : 2 * NOPE + ROPE, cols] = src[H * NOPE + i * ROPE : H * NOPE + (i + 1) * ROPE, :]
 
     def keys(slot):
-        lat = kvbuf[slot, :, :nk, :].reshape(X * nk, T).astype(F32)
-        rope = kvbuf[slot, :, nk : nk + 2 * RX, :].astype(F32)[:, :RX].reshape(ROPE, T)
+        lat = kvbuf[slot, :, c, :nk, :].reshape(X * nk, T).astype(F32)
+        rope = kvbuf[slot, :, c, nk : nk + 2 * RX, :].astype(F32)[:, :RX].reshape(ROPE, T)
         return lat, rope
 
     def chunk(slot_a, slot_b):
@@ -365,12 +378,23 @@
         own = off == HALF
         slot_a = at(-off)
         slot_b = jnp.where(own, z, at(off))
-        got_up(slot_a)
-        pl.when(own)(lambda: got_up(slot_b))
-        pl.when(jnp.logical_not(own))(lambda: got_dn(slot_b))
+
+        def take():
+            got_up(slot_a)
+            pl.when(own)(lambda: got_up(slot_b))
+            pl.when(jnp.logical_not(own))(lambda: got_dn(slot_b))
+            k_hand(slot_a).start()
+            k_hand(slot_b).start()
+
+        def handed():
+            k_hand(slot_a).wait_recv()
+            k_hand(slot_b).wait_recv()
+
+        pl.when(c == 0)(take)
+        pl.when(c == 1)(handed)
         chunk(slot_a, slot_b)
 
-    def step(i, _):
+    def transport(i):
         def stops_in():
             stop(i, 0)
             stop(i, 1)
@@ -385,11 +409,12 @@
         pl.when(i - 1 <= K)(relay_stops)
         pl.when(jnp.logical_and(i - 2 >= 0, i - 2 <= K))(lambda: leaves(i - 2, relay_up, relay_dn))
 
+    def step(i, _):
+        pl.when(c == 0)(lambda: transport(i))
         pl.when(i <= K + 1)(lambda: w_steps(W_FIRST + 1 + W_EACH * (i - 1), W_EACH))
-
         pl.when(i == 1)(make_q)
         pl.when(i == 2)(place_q)
-        pl.when(i == K + 1)(w_rest)
+        pl.when(i == K + 2)(w_rest)
 
         def one(r, _):
             j = jnp.where(r == 0, i - 2, i - 3)
@@ -500,14 +525,18 @@
         pl.when(j >= 1)(back)
         return 0
 
-    lax.fori_loop(0, K + 1, k_sent, 0)
-
     def sent_slots(s, _):
         for kind, dev in ((0, to_xr), (1, to_xl), (2, to_xr)):
             k_x(s, x, kind, dev).wait_send()
+        k_hand(s).wait_send()
         return 0
 
-    lax.fori_loop(0, Z, sent_slots, 0)
+    def k_all():
+        lax.fori_loop(0, K + 1, k_sent, 0)
+        lax.fori_loop(0, Z, sent_slots, 0)
+
+    pl.when(c == 0)(k_all)
+    pl.when(c == 1)(k_own.wait_send)
 
 
 def solution(mesh):
@@ -541,7 +570,7 @@
             V((X, nq, T), BF16),
             V((H * (NOPE + ROPE), T), BF16), V((H * (NOPE + ROPE), T), BF16),
             V((H // 2, 256, 4 * T), BF16),
-            V((Z, X, nk + 2 * RX, T), BF16),
+            V((Z, X, 2, nk + 2 * RX, T), BF16), V((nk + 2 * RX, T), BF16),
             V((ROPE, T), F32), V((2, ROPE, T), F32),
             V((nq * X, 128), F32), V((nk * X, 128), F32),
             V((T, 128), F32),
@@ -552,7 +581,7 @@
             DMA((13,)),
             DMA((6,)), DMA((6,)),
             DMA((3,)), DMA((3,)), DMA((1,)), DMA((1,)),
-            DMA((2, K)), DMA((Z, 2)), DMA((Z,)), DMA((Z, 3)), DMA((Z, 3)),
+            DMA((2, K)), DMA((Z, 2)), DMA((1,)), DMA((1,)), DMA((Z,)), DMA((Z,)), DMA((Z,)), DMA((Z, 3)), DMA((Z, 3)),
             DMA((2, Z // 2, 2)), DMA((Z, 2)), DMA((Z,)), DMA((Z,)), DMA((1,)), DMA((1,)),
             DMA((1,)), DMA((1,)), DMA((2,)), DMA((2,)), DMA((3,)), DMA((3,)),
         ]

time: 130 us -> 128 us (0.985)
  Pallas kernels: 126 us -> 123 us
    pallas_call x1, Pallas kernels: 126 us -> 123 us  [per_device(): pl.pallas_call(functools.partial(kernel, SP, X), out_shape=jax.ShapeDtype...]
where the time goes in v3:
time: 128 us; the launch traced here: 127 us
  Pallas kernels  123 us (96%)
  local copies, waits for them, and re-layouts  3.97 us (3%)
    pallas_call x1, Pallas kernels, per_device(): pl.pallas_call(functools.partial(kernel, SP, X), out_shape=jax.ShapeDtype...  123 us

profile of v3, /device:TPU:33, one launch (start us, length us, event | category | flops | bytes accessed | tf_op | source)
XLA Modules:
  0.0 127.5 jit_solution(13042343404339462499)
XLA Ops:
  0.0 0.0 copy-start
  0.0 0.0 copy-start.1
  0.0 1.2 reshape.11.kv_gain
  1.2 0.0 copy-done.1
  1.2 0.6 reshape.10.q_gain
  1.8 0.0 copy-done
  1.8 0.6 reshape.9.mix_gain
  2.4 123.5 %shard_map.163 = bf16[128,512]{1,0:T(8,128)(2,1)} custom-call(bf16[128,512]{1,0:T(8,128)(2,1)} %tokens.1, bf16[1,2048]{1,0:T(2,128)(2,1)} %reshape.9.mix_gain, bf16[32,256]{1,0:T(8,128)(2,1)} %wv.1, bf16[32,256]{1,0:T(8,128)(2,1)} %wo.1, bf16[32,256]{1,0:T(8,128)(2,1)} %wi.1, bf16[3,256]{1,0:T(4,128)(2,1)} %conv_kernel.1, bf16[2048,128]{1,0:T(8,128)(2,1)} %wqd.1, ...), custom_call_target="tpu_custom_call" | custom-call | tf_op jit(solution)/shard_map/pallas_call | solution.py:588
  125.9 1.6 %copy.19 = bf16[128,512]{1,0:T(8,128)(2,1)} copy(bf16[128,512]{1,0:T(8,128)(2,1)} %shard_map.163) | data formatting | bytes 262144
Async XLA Ops:
  0.0 1.8 %copy-start = (bf16[2048]{0:T(1024)(128)(2,1)S(1)}, bf16[2048]{0:T(1024)(128)(2,1)}, u32[]{:S(2)}) copy-start(bf16[2048]{0:T(1024)(128)(2,1)} %param.18) | copy-start | bytes 12292
  0.0 1.2 copy-start.1

commit v4 on v3

--- a/solution.py
+++ b/solution.py
@@ -18,8 +18,6 @@
 F32 = jnp.float32
 BF16 = jnp.bfloat16
 STRIDE = 3
-W_FIRST = 3
-W_EACH = 2
 
 
 def dot_f32(a, b, contract=((1,), (0,))):
@@ -34,7 +32,7 @@
     wbuf, tok, scaled, wqd_v, wd_t, wqn_v, wqr_v, wkn_v, wval_v, wval_t, wout,
     qbuf, qmine, qpart, qz, kvbuf, kv_mine, rope_scr, cs_scr, qg_col, kvg_col, rs_scr,
     o_acc, m_acc, l_acc, o_send, o_recv, gated, halo, yconv, rs_send, rs_recv,
-    loc, tk_s, tk_r, q_s, q_r, qp_s, qp_r, kf_s, kn_s, ko_s, ko_r, kh_s, kh_r, kz_r, kx_s, kx_r, wz_s, wz_r, wp_s, wp_r, wq_s, wq_r,
+    loc, tk_s, tk_r, q_s, q_r, qp_s, qp_r, kf_s, kn_s, ko_s, ko_r, kh_s, kh_r, kz_r, kx_s, kx_r, wf_s, wn_s, wz_r, wp_s, wp_r, wq_s, wq_r,
     o_s, o_r, h_s, h_r, r_s, r_r,
 ):
     Z = SP // 2
@@ -102,9 +100,25 @@
     for cp in tok_sends:
         cp.start()
 
-    def w_z(slot, d, way, core, dev):
+    def at(offset):
+        return lax.rem(z + offset + 2 * Z, Z)
+
+    def leaves(j, fn_up, fn_dn):
+        def inner():
+            fn_up(at(-STRIDE * j + 1))
+            fn_dn(at(STRIDE * j - 1))
+
+        fn_up(at(-STRIDE * j - 1))
+        pl.when(j < K)(lambda: fn_dn(at(STRIDE * j + 1)))
+        pl.when(j >= 1)(inner)
+
+    def w_far(slot, j, way, core):
         piece = wbuf.at[:, slot, core]
-        return remote(piece, piece, wz_s.at[way, d, core], wz_r.at[slot, core], dev)
+        return remote(piece, piece, wf_s.at[way, j, core], wz_r.at[slot, core], far_dn if way else far_up)
+
+    def w_near(slot, way, core):
+        piece = wbuf.at[:, slot, core]
+        return remote(piece, piece, wn_s.at[slot, way, core], wz_r.at[slot, core], to_dn if way else to_up)
 
     def w_p(slot):
         return remote(wbuf.at[:, slot], wbuf.at[:, slot], wp_s.at[slot], wp_r.at[slot], partner)
@@ -117,29 +131,42 @@
     w_own(c).start()
 
     def w_begin(core):
-        w_z(z, 0, 0, core, to_up).start()
-        w_z(z, 0, 1, core, to_dn).start()
+        for way in (0, 1):
+            w_far(z, 0, way, core).start()
+        for way in (0, 1):
+            w_near(z, way, core).start()
 
     pl.when(c == 1)(lambda: w_begin(1))
 
-    def w_in(k, way):
-        slot = lax.rem(z - k + Z, Z) if way == 0 else lax.rem(z + k, Z)
-        dev = to_up if way == 0 else to_dn
-        end = HALF if way == 0 else HALF - 1
+    def w_stop(j, way):
+        slot = at(STRIDE * j if way else -STRIDE * j)
         for core in (1, 0):
-            w_z(slot, k, way, core, dev).wait_recv()
-            pl.when(k < end)(lambda core=core: w_z(slot, k, way, core, dev).start())
+            w_near(slot, 0, core).wait_recv()
+            pl.when(j < K)(lambda core=core: w_far(slot, j, way, core).start())
+
+        def nears(to):
+            for core in (1, 0):
+                w_near(slot, to, core).start()
+
+        nears(0)
+        if way == 0:
+            nears(1)
+        else:
+            pl.when(j < K)(lambda: nears(1))
         w_p(slot).start()
 
-    def w_step(k):
-        pl.when(jnp.logical_and(c == 1, k <= HALF))(lambda: w_in(k, 0))
-        pl.when(jnp.logical_and(c == 1, k <= HALF - 1))(lambda: w_in(k, 1))
-
-    def w_steps(first, count):
-        def one(i, _):
-            w_step(first + i)
-            return 0
-        lax.fori_loop(0, count, one, 0)
+    def w_leaf(slot):
+        for core in (1, 0):
+            w_near(slot, 0, core).wait_recv()
+        w_p(slot).start()
+
+    def w_step(j):
+        def stops_in():
+            w_stop(j, 0)
+            w_stop(j, 1)
+
+        pl.when(jnp.logical_and(c == 1, j <= K))(stops_in)
+        pl.when(jnp.logical_and(c == 1, j <= K + 1))(lambda: leaves(j - 1, w_leaf, w_leaf))
 
     wd_t[nk + nr :, :] = jnp.zeros((wd_t.shape[0] - nk - nr, D), BF16)
     rows16 = lax.broadcasted_iota(jnp.int32, (ROPE, T), 0)
@@ -166,7 +193,7 @@
     tok_copy(5, xr, hi, to_xl, False).start()
     tok_copy(1, xl, hi, to_xr, False).wait_recv()
     tok_copy(3, xr, lo, to_xl, False).wait_recv()
-    w_steps(1, 1)
+    w_step(1)
     tok_copy(4, xo, lo, to_xr, False).wait_recv()
     tok_copy(5, xo, hi, to_xl, False).wait_recv()
     tok_cp.wait()
@@ -239,7 +266,7 @@
     for cp in q_sends:
         cp.start()
     pl.when(c == 0)(k_begin)
-    w_steps(2, W_FIRST - 1)
+    w_step(2)
 
     factor = (NOPE + ROPE) ** (-0.5) * LOG2E
     q_exchange = remote(qmine, qpart, qp_s.at[0], qp_r.at[0], partner)
@@ -325,9 +352,6 @@
         halo_copy(1, to_prev).start()
         yconv[...] = project(1)
 
-    def at(offset):
-        return lax.rem(z + offset + 2 * Z, Z)
-
     def spread(slot):
         k_x(slot, x, 0, to_xr).start()
         k_x(slot, x, 1, to_xl).start()
@@ -356,15 +380,6 @@
         k_x(slot, xr, 1, to_xl).wait_recv()
         k_x(slot, xr, 2, to_xl).start()
 
-    def leaves(j, fn_up, fn_dn):
-        def inner():
-            fn_up(at(-STRIDE * j + 1))
-            fn_dn(at(STRIDE * j - 1))
-
-        fn_up(at(-STRIDE * j - 1))
-        pl.when(j < K)(lambda: fn_dn(at(STRIDE * j + 1)))
-        pl.when(j >= 1)(inner)
-
     def got_up(slot):
         k_x(slot, xr, 1, to_xl).wait_recv()
         k_x(slot, xo, 2, to_xr).wait_recv()
@@ -411,10 +426,10 @@
 
     def step(i, _):
         pl.when(c == 0)(lambda: transport(i))
-        pl.when(i <= K + 1)(lambda: w_steps(W_FIRST + 1 + W_EACH * (i - 1), W_EACH))
+        w_step(i + 2)
         pl.when(i == 1)(make_q)
         pl.when(i == 2)(place_q)
-        pl.when(i == K + 2)(w_rest)
+        pl.when(i == K + 2)(conv_gates)
 
         def one(r, _):
             j = jnp.where(r == 0, i - 2, i - 3)
@@ -424,10 +439,6 @@
 
         lax.fori_loop(0, 3, one, 0)
         return 0
-
-    def w_rest():
-        w_steps(W_FIRST + 1 + W_EACH * (K + 1), HALF - W_FIRST - W_EACH * (K + 1))
-        conv_gates()
 
     lax.fori_loop(1, K + 4, step, 0)
 
@@ -491,15 +502,17 @@
 
     w_own(c).wait_send()
 
-    def w_sent(d, _):
+    def w_sent(j, _):
         for core in (0, 1):
-            w_z(z, d, 0, core, to_up).wait_send()
-
-        def back():
-            for core in (0, 1):
-                w_z(z, d, 1, core, to_dn).wait_send()
-
-        pl.when(d < HALF - 1)(back)
+            for way in (0, 1):
+                pl.when(j < K)(lambda way=way, core=core: w_far(z, j, way, core).wait_send())
+                w_near(at(-STRIDE * j), way, core).wait_send()
+
+            def back(core=core):
+                w_near(at(STRIDE * j), 0, core).wait_send()
+                pl.when(j < K)(lambda: w_near(at(STRIDE * j), 1, core).wait_send())
+
+            pl.when(j >= 1)(back)
         return 0
 
     def w_handed(i, _):
@@ -507,7 +520,7 @@
         return 0
 
     def w_all():
-        lax.fori_loop(0, HALF, w_sent, 0)
+        lax.fori_loop(0, K + 1, w_sent, 0)
         lax.fori_loop(1, Z, w_handed, 0)
 
     pl.when(c == 1)(w_all)
@@ -582,7 +595,7 @@
             DMA((6,)), DMA((6,)),
             DMA((3,)), DMA((3,)), DMA((1,)), DMA((1,)),
             DMA((2, K)), DMA((Z, 2)), DMA((1,)), DMA((1,)), DMA((Z,)), DMA((Z,)), DMA((Z,)), DMA((Z, 3)), DMA((Z, 3)),
-            DMA((2, Z // 2, 2)), DMA((Z, 2)), DMA((Z,)), DMA((Z,)), DMA((1,)), DMA((1,)),
+            DMA((2, K, 2)), DMA((Z, 2, 2)), DMA((Z, 2)), DMA((Z,)), DMA((Z,)), DMA((1,)), DMA((1,)),
             DMA((1,)), DMA((1,)), DMA((2,)), DMA((2,)), DMA((3,)), DMA((3,)),
         ]
         return pl.pallas_call(

time: 128 us -> 127 us (level)
  no operation moved by 1% of the time
where the time goes in v4:
time: 127 us; the launch traced here: 126 us
  Pallas kernels  122 us (96%)
  local copies, waits for them, and re-layouts  3.97 us (3%)
    pallas_call x1, Pallas kernels, per_device(): pl.pallas_call(functools.partial(kernel, SP, X), out_shape=jax.ShapeDtype...  122 us

profile of v4, /device:TPU:33, one launch (start us, length us, event | category | flops | bytes accessed | tf_op | source)
XLA Modules:
  0.0 126.3 jit_solution(2435814059763253731)
XLA Ops:
  0.0 0.0 copy-start
  0.0 0.0 copy-start.1
  0.0 1.2 reshape.11.kv_gain
  1.2 0.0 copy-done.1
  1.2 0.6 reshape.10.q_gain
  1.8 0.0 copy-done
  1.8 0.6 reshape.9.mix_gain
  2.4 122.3 %shard_map.163 = bf16[128,512]{1,0:T(8,128)(2,1)} custom-call(bf16[128,512]{1,0:T(8,128)(2,1)} %tokens.1, bf16[1,2048]{1,0:T(2,128)(2,1)} %reshape.9.mix_gain, bf16[32,256]{1,0:T(8,128)(2,1)} %wv.1, bf16[32,256]{1,0:T(8,128)(2,1)} %wo.1, bf16[32,256]{1,0:T(8,128)(2,1)} %wi.1, bf16[3,256]{1,0:T(4,128)(2,1)} %conv_kernel.1, bf16[2048,128]{1,0:T(8,128)(2,1)} %wqd.1, ...), custom_call_target="tpu_custom_call" | custom-call | tf_op jit(solution)/shard_map/pallas_call | solution.py:601
  124.8 1.6 %copy.19 = bf16[128,512]{1,0:T(8,128)(2,1)} copy(bf16[128,512]{1,0:T(8,128)(2,1)} %shard_map.163) | data formatting | bytes 262144
Async XLA Ops:
  0.0 1.8 %copy-start = (bf16[2048]{0:T(1024)(128)(2,1)S(1)}, bf16[2048]{0:T(1024)(128)(2,1)}, u32[]{:S(2)}) copy-start(bf16[2048]{0:T(1024)(128)(2,1)} %param.18) | copy-start | bytes 12292
  0.0 1.2 copy-start.1

commit v5 on v4

--- a/solution.py
+++ b/solution.py
@@ -18,6 +18,8 @@
 F32 = jnp.float32
 BF16 = jnp.bfloat16
 STRIDE = 3
+KC = 1
+WC = 0
 
 
 def dot_f32(a, b, contract=((1,), (0,))):
@@ -136,16 +138,16 @@
         for way in (0, 1):
             w_near(z, way, core).start()
 
-    pl.when(c == 1)(lambda: w_begin(1))
+    pl.when(c == WC)(lambda: w_begin(WC))
 
     def w_stop(j, way):
         slot = at(STRIDE * j if way else -STRIDE * j)
-        for core in (1, 0):
+        for core in (WC, 1 - WC):
             w_near(slot, 0, core).wait_recv()
             pl.when(j < K)(lambda core=core: w_far(slot, j, way, core).start())
 
         def nears(to):
-            for core in (1, 0):
+            for core in (WC, 1 - WC):
                 w_near(slot, to, core).start()
 
         nears(0)
@@ -156,7 +158,7 @@
         w_p(slot).start()
 
     def w_leaf(slot):
-        for core in (1, 0):
+        for core in (WC, 1 - WC):
             w_near(slot, 0, core).wait_recv()
         w_p(slot).start()
 
@@ -165,8 +167,8 @@
             w_stop(j, 0)
             w_stop(j, 1)
 
-        pl.when(jnp.logical_and(c == 1, j <= K))(stops_in)
-        pl.when(jnp.logical_and(c == 1, j <= K + 1))(lambda: leaves(j - 1, w_leaf, w_leaf))
+        pl.when(jnp.logical_and(c == WC, j <= K))(stops_in)
+        pl.when(jnp.logical_and(c == WC, j <= K + 1))(lambda: leaves(j - 1, w_leaf, w_leaf))
 
     wd_t[nk + nr :, :] = jnp.zeros((wd_t.shape[0] - nk - nr, D), BF16)
     rows16 = lax.broadcasted_iota(jnp.int32, (ROPE, T), 0)
@@ -186,7 +188,7 @@
     wval_t[...] = jnp.transpose(wval_v[...].astype(F32)).astype(BF16)
 
     w_own(1 - c).wait_recv()
-    pl.when(c == 1)(lambda: w_begin(0))
+    pl.when(c == WC)(lambda: w_begin(1 - WC))
     tok_copy(0, xl, lo, to_xr, False).wait_recv()
     tok_copy(4, xl, lo, to_xr, False).start()
     tok_copy(2, xr, hi, to_xl, False).wait_recv()
@@ -225,13 +227,13 @@
     RX = ROPE // X
     mine = rope_scr[pl.ds(pl.multiple_of(x * RX, RX), RX), :]
     kv_mine[nk:, :] = jnp.concatenate([mine, jnp.zeros((RX, T), F32)], axis=0).astype(BF16)
-    k_own = remote(kv_mine, kvbuf.at[z, x, 1], ko_s.at[0], ko_r.at[0], partner)
-    pl.when(c == 1)(k_own.start)
+    k_own = remote(kv_mine, kvbuf.at[z, x, 1 - KC], ko_s.at[0], ko_r.at[0], partner)
+    pl.when(c != KC)(k_own.start)
 
     def keep_mine():
-        kvbuf[z, x, 0] = kv_mine[...]
-
-    pl.when(c == 0)(keep_mine)
+        kvbuf[z, x, KC] = kv_mine[...]
+
+    pl.when(c == KC)(keep_mine)
 
     def k_far(slot, j, way):
         piece = kvbuf.at[slot, x]
@@ -245,7 +247,7 @@
         return remote(kvbuf.at[slot, piece], kvbuf.at[slot, piece], kx_s.at[slot, kind], kx_r.at[slot, kind], dev)
 
     def k_hand(slot):
-        return remote(kvbuf.at[slot, :, 1], kvbuf.at[slot, :, 1], kh_s.at[slot], kh_r.at[slot], partner)
+        return remote(kvbuf.at[slot, :, 1 - KC], kvbuf.at[slot, :, 1 - KC], kh_s.at[slot], kh_r.at[slot], partner)
 
     def k_begin():
         k_own.wait_recv()
@@ -265,7 +267,7 @@
     q_sends = [q_copy(2, x, to_xo), q_copy(0, x, to_xr), q_copy(1, x, to_xl)]
     for cp in q_sends:
         cp.start()
-    pl.when(c == 0)(k_begin)
+    pl.when(c == KC)(k_begin)
     w_step(2)
 
     factor = (NOPE + ROPE) ** (-0.5) * LOG2E
@@ -340,7 +342,7 @@
         def all_in():
             lax.fori_loop(1, Z, got, 0)
 
-        pl.when(c == 0)(all_in)
+        pl.when(c != WC)(all_in)
 
         def project(i):
             w = wbuf[i].reshape(D, wbuf.shape[-1])
@@ -405,8 +407,8 @@
             k_hand(slot_a).wait_recv()
             k_hand(slot_b).wait_recv()
 
-        pl.when(c == 0)(take)
-        pl.when(c == 1)(handed)
+        pl.when(c == KC)(take)
+        pl.when(c != KC)(handed)
         chunk(slot_a, slot_b)
 
     def transport(i):
@@ -425,7 +427,7 @@
         pl.when(jnp.logical_and(i - 2 >= 0, i - 2 <= K))(lambda: leaves(i - 2, relay_up, relay_dn))
 
     def step(i, _):
-        pl.when(c == 0)(lambda: transport(i))
+        pl.when(c == KC)(lambda: transport(i))
         w_step(i + 2)
         pl.when(i == 1)(make_q)
         pl.when(i == 2)(place_q)
@@ -485,6 +487,62 @@
         rs_send[rel] = dot_f32(y, wout[:, cols]).astype(BF16)
         if dev is not None:
             remote(rs_send.at[rel], rs_recv.at[rel - 1], r_s.at[rel - 1], r_r.at[rel - 1], dev).start()
+    for cp in tok_sends + [tok_copy(4, xl, lo, to_xr, False), tok_copy(5, xr, hi, to_xl, False)]:
+        cp.wait_send()
+    for cp in q_sends + [q_exchange, halo_copy(0, to_next), halo_copy(1, to_prev), o_exchange]:
+        cp.wait_send()
+
+    w_own(c).wait_send()
+
+    def w_sent(j, _):
+        for core in (0, 1):
+            for way in (0, 1):
+                pl.when(j < K)(lambda way=way, core=core: w_far(z, j, way, core).wait_send())
+                w_near(at(-STRIDE * j), way, core).wait_send()
+
+            def back(core=core):
+                w_near(at(STRIDE * j), 0, core).wait_send()
+                pl.when(j < K)(lambda: w_near(at(STRIDE * j), 1, core).wait_send())
+
+            pl.when(j >= 1)(back)
+        return 0
+
+    def w_handed(i, _):
+        w_p(lax.rem(z + i, Z)).wait_send()
+        return 0
+
+    def w_all():
+        lax.fori_loop(0, K + 1, w_sent, 0)
+        lax.fori_loop(1, Z, w_handed, 0)
+
+    pl.when(c == WC)(w_all)
+
+    def k_sent(j, _):
+        for way in (0, 1):
+            pl.when(j < K)(lambda way=way: k_far(z, j, way).wait_send())
+        k_near(at(-STRIDE * j), 0).wait_send()
+        k_near(at(-STRIDE * j), 1).wait_send()
+
+        def back():
+            k_near(at(STRIDE * j), 0).wait_send()
+            pl.when(j < K)(lambda: k_near(at(STRIDE * j), 1).wait_send())
+
+        pl.when(j >= 1)(back)
+        return 0
+
+    def sent_slots(s, _):
+        for kind, dev in ((0, to_xr), (1, to_xl), (2, to_xr)):
+            k_x(s, x, kind, dev).wait_send()
+        k_hand(s).wait_send()
+        return 0
+
+    def k_all():
+        lax.fori_loop(0, K + 1, k_sent, 0)
+        lax.fori_loop(0, Z, sent_slots, 0)
+
+    pl.when(c == KC)(k_all)
+    pl.when(c != KC)(k_own.wait_send)
+
     total = rs_send[0].astype(F32)
     r_copies = [
         remote(rs_send.at[rel], rs_recv.at[rel - 1], r_s.at[rel - 1], r_r.at[rel - 1], dev)
@@ -494,62 +552,8 @@
         cp.wait_recv()
         total += rs_recv[rel - 1].astype(F32)
     out[...] = total.astype(BF16)
-
-    for cp in tok_sends + [tok_copy(4, xl, lo, to_xr, False), tok_copy(5, xr, hi, to_xl, False)]:
+    for cp in r_copies:
         cp.wait_send()
-    for cp in q_sends + [q_exchange, halo_copy(0, to_next), halo_copy(1, to_prev), o_exchange] + r_copies:
-        cp.wait_send()
-
-    w_own(c).wait_send()
-
-    def w_sent(j, _):
-        for core in (0, 1):
-            for way in (0, 1):
-                pl.when(j < K)(lambda way=way, core=core: w_far(z, j, way, core).wait_send())
-                w_near(at(-STRIDE * j), way, core).wait_send()
-
-            def back(core=core):
-                w_near(at(STRIDE * j), 0, core).wait_send()
-                pl.when(j < K)(lambda: w_near(at(STRIDE * j), 1, core).wait_send())
-
-            pl.when(j >= 1)(back)
-        return 0
-
-    def w_handed(i, _):
-        w_p(lax.rem(z + i, Z)).wait_send()
-        return 0
-
-    def w_all():
-        lax.fori_loop(0, K + 1, w_sent, 0)
-        lax.fori_loop(1, Z, w_handed, 0)
-
-    pl.when(c == 1)(w_all)
-
-    def k_sent(j, _):
-        for way in (0, 1):
-            pl.when(j < K)(lambda way=way: k_far(z, j, way).wait_send())
-        k_near(at(-STRIDE * j), 0).wait_send()
-        k_near(at(-STRIDE * j), 1).wait_send()
-
-        def back():
-            k_near(at(STRIDE * j), 0).wait_send()
-            pl.when(j < K)(lambda: k_near(at(STRIDE * j), 1).wait_send())
-
-        pl.when(j >= 1)(back)
-        return 0
-
-    def sent_slots(s, _):
-        for kind, dev in ((0, to_xr), (1, to_xl), (2, to_xr)):
-            k_x(s, x, kind, dev).wait_send()
-        k_hand(s).wait_send()
-        return 0
-
-    def k_all():
-        lax.fori_loop(0, K + 1, k_sent, 0)
-        lax.fori_loop(0, Z, sent_slots, 0)
-
-    pl.when(c == 0)(k_all)
-    pl.when(c == 1)(k_own.wait_send)
 
 
 def solution(mesh):

time: 127 us -> 129 us (1.016)
  Pallas kernels: 122 us -> 125 us
    pallas_call x1, Pallas kernels: 122 us -> 125 us  [per_device(): pl.pallas_call(functools.partial(kernel, SP, X), out_shape=jax.ShapeDtype...]
where the time goes in v5:
time: 129 us
  Pallas kernels  125 us (97%)
  local copies, waits for them, and re-layouts  3.97 us (3%)
    pallas_call x1, Pallas kernels, per_device(): pl.pallas_call(functools.partial(kernel, SP, X), out_shape=jax.ShapeDtype...  125 us

profile of v5, /device:TPU:33, one launch (start us, length us, event | category | flops | bytes accessed | tf_op | source)
XLA Modules:
  0.0 129.0 jit_solution(2571037481520563139)
XLA Ops:
  0.0 0.0 copy-start
  0.0 0.0 copy-start.1
  0.0 1.2 reshape.11.kv_gain
  1.2 0.0 copy-done.1
  1.2 0.6 reshape.10.q_gain
  1.8 0.0 copy-done
  1.8 0.6 reshape.9.mix_gain
  2.4 125.0 %shard_map.163 = bf16[128,512]{1,0:T(8,128)(2,1)} custom-call(bf16[128,512]{1,0:T(8,128)(2,1)} %tokens.1, bf16[1,2048]{1,0:T(2,128)(2,1)} %reshape.9.mix_gain, bf16[32,256]{1,0:T(8,128)(2,1)} %wv.1, bf16[32,256]{1,0:T(8,128)(2,1)} %wo.1, bf16[32,256]{1,0:T(8,128)(2,1)} %wi.1, bf16[3,256]{1,0:T(4,128)(2,1)} %conv_kernel.1, bf16[2048,128]{1,0:T(8,128)(2,1)} %wqd.1, ...), custom_call_target="tpu_custom_call" | custom-call | tf_op jit(solution)/shard_map/pallas_call | solution.py:605
  127.4 1.6 %copy.19 = bf16[128,512]{1,0:T(8,128)(2,1)} copy(bf16[128,512]{1,0:T(8,128)(2,1)} %shard_map.163) | data formatting | bytes 262144
Async XLA Ops:
  0.0 1.8 %copy-start = (bf16[2048]{0:T(1024)(128)(2,1)S(1)}, bf16[2048]{0:T(1024)(128)(2,1)}, u32[]{:S(2)}) copy-start(bf16[2048]{0:T(1024)(128)(2,1)} %param.18) | copy-start | bytes 12292
  0.0 1.2 copy-start.1

commit v6 on v5

--- a/solution.py
+++ b/solution.py
@@ -18,8 +18,8 @@
 F32 = jnp.float32
 BF16 = jnp.bfloat16
 STRIDE = 3
-KC = 1
-WC = 0
+KC = 0
+WC = 1
 
 
 def dot_f32(a, b, contract=((1,), (0,))):

time: 129 us -> 126 us (0.977)
  Pallas kernels: 125 us -> 122 us
    pallas_call x1, Pallas kernels: 125 us -> 122 us  [per_device(): pl.pallas_call(functools.partial(kernel, SP, X), out_shape=jax.ShapeDtype...]
where the time goes in v6:
time: 126 us
  Pallas kernels  122 us (97%)
  local copies, waits for them, and re-layouts  3.97 us (3%)
    pallas_call x1, Pallas kernels, per_device(): pl.pallas_call(functools.partial(kernel, SP, X), out_shape=jax.ShapeDtype...  122 us

profile of v6, /device:TPU:33, one launch (start us, length us, event | category | flops | bytes accessed | tf_op | source)
XLA Modules:
  0.0 125.7 jit_solution(5126049255714471505)
XLA Ops:
  0.0 0.0 copy-start
  0.0 0.0 copy-start.1
  0.0 1.2 reshape.11.kv_gain
  1.2 0.0 copy-done.1
  1.2 0.6 reshape.10.q_gain
  1.8 0.0 copy-done
  1.8 0.6 reshape.9.mix_gain
  2.4 121.7 %shard_map.163 = bf16[128,512]{1,0:T(8,128)(2,1)} custom-call(bf16[128,512]{1,0:T(8,128)(2,1)} %tokens.1, bf16[1,2048]{1,0:T(2,128)(2,1)} %reshape.9.mix_gain, bf16[32,256]{1,0:T(8,128)(2,1)} %wv.1, bf16[32,256]{1,0:T(8,128)(2,1)} %wo.1, bf16[32,256]{1,0:T(8,128)(2,1)} %wi.1, bf16[3,256]{1,0:T(4,128)(2,1)} %conv_kernel.1, bf16[2048,128]{1,0:T(8,128)(2,1)} %wqd.1, ...), custom_call_target="tpu_custom_call" | custom-call | tf_op jit(solution)/shard_map/pallas_call | solution.py:605
  124.2 1.6 %copy.19 = bf16[128,512]{1,0:T(8,128)(2,1)} copy(bf16[128,512]{1,0:T(8,128)(2,1)} %shard_map.163) | data formatting | bytes 262144
Async XLA Ops:
  0.0 1.8 %copy-start = (bf16[2048]{0:T(1024)(128)(2,1)S(1)}, bf16[2048]{0:T(1024)(128)(2,1)}, u32[]{:S(2)}) copy-start(bf16[2048]{0:T(1024)(128)(2,1)} %param.18) | copy-start | bytes 12292
  0.0 1.2 copy-start.1
